TPU v7x, 256 devices: a whole 4x4x8 slice. The times are simulated.
256 devices in a mesh: fs: 32 (over z, x), tp: 8 (over y, core).
Axes of the slice: x: 4, y: 4, z: 8, core: 2. Of those that a mesh axis runs over, the one named last changes fastest.
Arguments:
- later_input: bfloat16 [32768, 2048], P(('fs', 'tp')), may hold values from -6 to 6
- saved_input: bfloat16 [32768, 2048], P(('fs', 'tp')), may hold values from -24 to 24
- cotangent: bfloat16 [32768, 3072], P('fs', 'tp'), may hold values from -6 to 6
- up_weight: bfloat16 [2048, 3072], P('fs', 'tp'), may hold values from -0.125 to 0.125
- gate_weight: bfloat16 [2048, 3072], P('fs', 'tp'), may hold values from -0.125 to 0.125
- up_taps: bfloat16 [3, 3072], replicated, may hold values from -3.5 to 3.5
- gate_taps: bfloat16 [3, 3072], replicated, may hold values from -3.5 to 3.5
- up_grad_sum: float32 [2048, 3072], P('fs', 'tp'), may hold values from -6 to 6
- gate_grad_sum: float32 [2048, 3072], P('fs', 'tp'), may hold values from -6 to 6
- up_taps_sum: float32 [3, 3072], replicated, may hold values from -6 to 6
- gate_taps_sum: float32 [3, 3072], replicated, may hold values from -6 to 6
Outputs:
- hidden: bfloat16 [32768, 3072], P('fs', 'tp')
- input_grad: bfloat16 [32768, 2048], P(('fs', 'tp'))
- new_up_sum: float32 [2048, 3072], P('fs', 'tp')
- new_gate_sum: float32 [2048, 3072], P('fs', 'tp')
- new_up_taps_sum: float32 [3, 3072], replicated
- new_gate_taps_sum: float32 [3, 3072], replicated
All inputs are finite; a program needn't handle non-finite values.
Results may differ from a plain program's by a relative error of at most 0.018.
Values may be sent and summed in bfloat16 or wider, within the bound.
No kernel may reach another device: no remote copies, remote signals or barrier semaphores. Data moves between devices by JAX's collectives and lax.ppermute only.
A program may use at most 64 MiB of HBM per device.

v0:
```python
import jax
import jax.numpy as jnp
from jax import lax
from jax.sharding import Mesh
from jax.sharding import PartitionSpec as P

TP = ("tp_0", "tp_1")
FS = ("fs_0", "fs_1")
FS_TP = ("fs_0", "fs_1", "tp_0", "tp_1")


def sent_together(arrays, axis, dim, along):
    ends, at = ([], 0)
    for a in arrays[:-1]:
        at += a.shape[along]
        ends.append(at)
    both = jnp.concatenate(arrays, axis=along)
    return tuple(jnp.split(lax.all_gather(both, axis, axis=dim, tiled=True), ends, axis=along))


def in_order(tiles, dim):
    tiles = jnp.moveaxis(tiles, 0, dim)
    dims = tiles.shape
    return tiles.reshape(*dims[:dim], dims[dim] * dims[dim + 1], *dims[dim + 2 :])


def sent_to_all(array, axis):
    peers = lax.axis_size(axis)
    return lax.all_to_all(
        jnp.broadcast_to(array[None], (peers, *array.shape)), axis, 0, 0, tiled=True
    )


def collect(array, axis, dim):
    return in_order(sent_to_all(array, axis), dim)


def split_up(array, dim, peers):
    before, after = (array.shape[:dim], array.shape[dim + 1 :])
    return jnp.moveaxis(array.reshape(*before, peers, -1, *after), dim, 0)


def summed_on_arrival(array, axis, dim):
    peers = lax.axis_size(axis)
    tiles = lax.all_to_all(split_up(array, dim, peers), axis, 0, 0, tiled=True)
    return jnp.sum(tiles, axis=0)


def sum_by_axis(array, axes, dim):
    far, near = axes
    own = summed_on_arrival(split_up(array, dim, lax.axis_size(far)), near, dim + 1)
    return jnp.sum(lax.all_to_all(own, far, 0, 0, tiled=True), axis=0)


def filled_up(lines, peers):
    spare = -lines.shape[0] % peers
    if not spare:
        return lines
    return jnp.concatenate([lines, jnp.zeros((spare, *lines.shape[1:]), lines.dtype)])


def whole_of(array, axes, dim):
    far, near = axes
    tiles = sent_to_all(sent_to_all(array, far), near)
    return in_order(tiles.swapaxes(0, 1).reshape(-1, *array.shape), dim)


def nested_sum(array, axes):
    own = sum_by_axis(filled_up(array, lax.axis_size(axes[0]) * lax.axis_size(axes[1])), axes, 0)
    whole = whole_of(own, axes, 0)
    return whole[: len(array)].reshape(array.shape)


def packed_total(arrays, axis):
    ends = [0]
    for a in arrays:
        ends.append(ends[-1] + a.size)
    subtotal = nested_sum(jnp.concatenate([a.ravel() for a in arrays]), axis)
    return tuple((subtotal[b:e].reshape(a.shape) for a, b, e in zip(arrays, ends, ends[1:])))


def summed_rows(terms, axes):
    subtotal = terms.astype(jnp.bfloat16)
    for axis in axes:
        subtotal = lax.psum_scatter(subtotal, axis, scatter_dimension=0, tiled=True)
    return subtotal.astype(jnp.float32)


def sent_and_summed(array, axis, dim):
    tiles = split_up(array, dim, lax.axis_size(axis))
    arrived = lax.all_to_all(tiles, axis, split_axis=0, concat_axis=0, tiled=True)
    return arrived.astype(jnp.float32).sum(axis=0)


def sum_in_two_steps(array, axes, dim):
    far, near = axes
    own = sent_and_summed(split_up(array, dim, lax.axis_size(far)), near, dim + 1)
    return jnp.sum(
        lax.all_to_all(own.astype(jnp.bfloat16), far, 0, 0, tiled=True).astype(jnp.float32), axis=0
    )


def delayed(values, steps):
    zeros = jnp.zeros_like(values[:steps])
    return jnp.concatenate([zeros, values[:-steps]], axis=0)


def advanced(values, steps):
    zeros = jnp.zeros_like(values[:steps])
    return jnp.concatenate([values[steps:], zeros], axis=0)


def depthwise(values, taps):
    return taps[2] * values + taps[1] * delayed(values, 1) + taps[0] * delayed(values, 2)


def depthwise_back(grads, taps):
    return taps[2] * grads + taps[1] * advanced(grads, 1) + taps[0] * advanced(grads, 2)


def taps_grad(grads, values):
    return jnp.stack(
        [
            jnp.sum(grads * delayed(values, 2), axis=0),
            jnp.sum(grads * delayed(values, 1), axis=0),
            jnp.sum(grads * values, axis=0),
        ],
        axis=0,
    )


def make_term(rows_all, grads):
    return lax.dot_general(
        rows_all, grads, (((0,), (0,)), ((), ())), preferred_element_type=jnp.float32
    )


def shards(
    later_input,
    saved_input,
    cotangent,
    up_weight,
    gate_weight,
    up_taps,
    gate_taps,
    up_grad_sum,
    gate_grad_sum,
    up_taps_sum,
    gate_taps_sum,
):
    column_count = up_weight.shape[1]
    group_size = lax.axis_size(TP)
    offset = lax.axis_index(TP) * column_count
    tokens_all = later_input.shape[0] * lax.axis_size(FS) * group_size
    grad_scale = jnp.float32(tokens_all ** (-0.5))
    taps_both = jnp.concatenate(
        [
            lax.dynamic_slice_in_dim(up_taps, offset, column_count, 1),
            lax.dynamic_slice_in_dim(gate_taps, offset, column_count, 1),
        ],
        axis=1,
    ).astype(jnp.float32)
    weight_both = jnp.concatenate([up_weight, gate_weight], axis=1)
    later_rows, saved_rows = sent_together((later_input, saved_input), TP, 0, 1)
    whole_weights = collect(weight_both, FS, 0)
    proj_later = jnp.dot(later_rows, whole_weights, preferred_element_type=jnp.float32)
    proj_saved = jnp.dot(saved_rows, whole_weights, preferred_element_type=jnp.float32)
    conv_later = depthwise(proj_later.astype(jnp.bfloat16).astype(jnp.float32), taps_both)
    hidden = (jax.nn.silu(conv_later[:, column_count:]) * conv_later[:, :column_count]).astype(
        jnp.bfloat16
    )
    saved_proj = proj_saved.astype(jnp.bfloat16)
    saved_proj32 = saved_proj.astype(jnp.float32)
    conv_saved = depthwise(saved_proj32, taps_both)
    saved_up = conv_saved[:, :column_count]
    saved_gate = conv_saved[:, column_count:]
    sigmoid_gate = jax.nn.sigmoid(saved_gate)
    upstream = cotangent.astype(jnp.float32)
    grad_conv = jnp.concatenate(
        [
            upstream * jax.nn.silu(saved_gate),
            upstream * saved_up * sigmoid_gate * (1.0 + saved_gate * (1.0 - sigmoid_gate)),
        ],
        axis=1,
    )
    grad_proj = depthwise_back(grad_conv, taps_both).astype(jnp.bfloat16)
    taps_local = taps_grad(grad_conv, saved_proj32)
    total_cols = column_count * group_size
    taps_up_full = lax.dynamic_update_slice_in_dim(
        jnp.zeros((3, total_cols), jnp.float32), taps_local[:, :column_count], offset, 1
    )
    taps_gate_full = lax.dynamic_update_slice_in_dim(
        jnp.zeros((3, total_cols), jnp.float32), taps_local[:, column_count:], offset, 1
    )
    taps_up_total, taps_gate_total = packed_total(
        (taps_up_full, taps_gate_full), (("fs_0", "fs_1"), ("tp_0", "tp_1"))
    )
    weight_grad = summed_rows(make_term(saved_rows, grad_proj), FS)
    up_grad = weight_grad[:, :column_count]
    gate_grad = weight_grad[:, column_count:]
    input_grad = sum_in_two_steps(
        lax.dot_general(
            grad_proj, whole_weights, (((1,), (1,)), ((), ())), preferred_element_type=jnp.float32
        ).astype(jnp.bfloat16),
        ("tp_0", "tp_1"),
        0,
    )
    new_up_sum = up_grad_sum + grad_scale * up_grad
    new_gate_sum = gate_grad_sum + grad_scale * gate_grad
    new_up_taps_sum = up_taps_sum + grad_scale * taps_up_total
    new_gate_taps_sum = gate_taps_sum + grad_scale * taps_gate_total
    return (
        hidden,
        input_grad.astype(jnp.bfloat16),
        new_up_sum,
        new_gate_sum,
        new_up_taps_sum,
        new_gate_taps_sum,
    )


def solution(mesh):
    finer = Mesh(mesh.devices.reshape(8, 4, 4, 2), ("fs_0", "fs_1", "tp_0", "tp_1"))
    in_specs = (
        P(FS_TP, None),
        P(FS_TP, None),
        P(FS, TP),
        P(FS, TP),
        P(FS, TP),
        P(),
        P(),
        P(FS, TP),
        P(FS, TP),
        P(),
        P(),
    )
    out_specs = (P(FS, TP), P(FS_TP, None), P(FS, TP), P(FS, TP), P(), P())
    return jax.shard_map(
        shards, mesh=finer, in_specs=in_specs, out_specs=out_specs, check_vma=False
    )
```

profile of v0, /device:TPU:1, one launch (start us, length us, event | category | flops | bytes accessed | tf_op | source)
XLA Modules:
  0.0 230.7 jit_solution(6842859936598074910)
XLA Ops:
  7.2 0.0 copy-start.6
  7.2 0.0 copy-start.5
  7.2 0.0 all-gather.2.cloned.1.call-start
  7.2 2.3 pad_maximum_fusion.1
  9.5 0.0 all-gather.2.cloned.1.call-update
  9.5 0.0 copy-done.6
  9.5 0.0 copy-done.5
  9.6 2.1 broadcast_in_dim.8
  11.7 11.9 %all-to-all-start = ((bf16[32,64,768]{2,1,0:T(8,128)(2,1)}), bf16[32,64,768]{2,1,0:T(8,128)(2,1)S(1)}, u32[]{:S(2)}, u32[]{:S(2)}) async-start(bf16[32,64,768]{2,1,0:T(8,128)(2,1)} %broadcast_in_dim.8), calls=%async_computation | async-start | bytes 6291456 | tf_op jit(solution)/shard_map/all_to_all | solution.py:29
  23.6 0.0 reduce-scatter.3.cloned.1.call-start
  23.6 0.7 constant_dynamic-slice_fusion
  24.4 69.5 %all-to-all-done = bf16[32,64,768]{2,1,0:T(8,128)(2,1)S(1)} async-done(((bf16[32,64,768]{2,1,0:T(8,128)(2,1)}), bf16[32,64,768]{2,1,0:T(8,128)(2,1)S(1)}, u32[]{:S(2)}, u32[]{:S(2)}) %all-to-all-start) | async-done | bytes 3145760 | tf_op jit(solution)/shard_map/all_to_all | solution.py:29
  93.9 6.3 %fusion.14 = f32[1024,768]{1,0:T(8,128)S(1)} fusion(bf16[2048,768]{1,0:T(8,128)(2,1)S(1)} %bitcast.27, bf16[1024,4096]{1,0:T(8,128)(2,1)} %all-gather.2.cloned.1.call-done), kind=kOutput, calls=%fused_computation.25 | convolution fusion | flops 3222798336 | bytes 10485760 | tf_op jit(solution)/shard_map/dot_general | solution.py:167
  100.2 0.0 copy-start.2
  100.2 0.9 multiply_add_fusion
  101.1 0.2 copy-done.2
  101.3 0.9 fusion.24
  102.2 0.0 slice-start.1
  102.2 0.2 fusion.9
  102.5 0.2 fusion.10
  102.7 0.0 copy-done
  102.7 0.8 slice-done
  103.5 1.5 slice-done.1
  105.0 3.4 %fusion.20 = f32[1024,768]{1,0:T(8,128)S(1)} fusion(bf16[2048,768]{1,0:T(8,128)(2,1)S(1)} %bitcast.28, bf16[1024,4096]{1,0:T(8,128)(2,1)S(1)} %bitcast.33), kind=kOutput, calls=%fused_computation.27 | convolution fusion | flops 3222798336 | bytes 10485760 | tf_op jit(solution)/shard_map/dot_general | solution.py:166
  108.4 4.9 %multiply_reduce_fusion.2 = (f32[768]{0:T(1024)S(1)}, f32[768]{0:T(1024)S(1)}, f32[768]{0:T(1024)S(1)}, bf16[1024,768]{1,0:T(8,128)(2,1)S(1)}, f32[1024,768]{1,0:T(8,128)S(1)}) fusion(f32[1022,768]{1,0:T(8,128)S(1)} %bitcast.21, f32[1024,384]{1,0:T(8,128)S(1)} %get-tuple-element.12, f32[1024,384]{1,0:T(8,128)S(1)} %get-tuple-element.13, ...), kind=kLoop, calls=%fused_computation.18 | loop fusion | flops 14153472 | bytes 33020928 | tf_op jit(solution)/shard_map/reduce_sum | solution.py:124
  113.3 0.0 copy-start.1
  113.3 1.2 copy-done.1
  114.5 7.5 %fusion.6 = bf16[2048,768]{1,0:T(8,128)(2,1)} fusion(bf16[1024,768]{1,0:T(8,128)(2,1)S(1)} %get-tuple-element.14, bf16[1024,4096]{1,0:T(8,128)(2,1)} %all-gather.2.cloned.1.call-done), kind=kOutput, calls=%fused_computation.13 | convolution fusion | flops 3222798336 | bytes 8912896 | tf_op jit(solution)/shard_map/dot_general | solution.py:133
  122.0 0.0 reduce-scatter.3.cloned.1.call-update
  122.1 0.1 concatenate.50
  122.3 0.1 concatenate.51
  122.4 12.4 %all_to_all.41 = f32[8,32,72]{2,1,0:T(8,128)S(1)} all-to-all(f32[8,32,72]{2,1,0:T(8,128)S(1)} %copy.23), channel_id=1, replica_groups=mesh['fs_0'=8,'fs_1'=4,'tp_0'=4,'tp_1'=2] {'tp_0','tp_1'}, dimensions={0} | all-to-all | bytes 147456 | tf_op jit(solution)/shard_map/all_to_all | solution.py:45
  134.9 0.6 reduce_sum.74
  135.5 6.0 %all-to-all-start.4 = ((f32[32,1,72]{2,1,0:T(1,128)}), f32[32,1,72]{2,1,0:T(1,128)S(1)}, u32[]{:S(2)}, u32[]{:S(2)}) async-start(f32[32,1,72]{2,1,0:T(1,128)} %bitcast.4), calls=%async_computation.6 | async-start | bytes 32768 | tf_op jit(solution)/shard_map/all_to_all | solution.py:52
  141.5 5.9 %convolution_convert_fusion = bf16[1024,2048]{1,0:T(8,128)(2,1)S(1)} fusion(bf16[1024,768]{1,0:T(8,128)(2,1)} %copy-done.1, bf16[2048,768]{1,0:T(8,128)(2,1)} %bitcast.29), kind=kOutput, calls=%fused_computation.8 | convolution fusion | flops 3223322624 | bytes 8912896 | tf_op jit(solution)/shard_map/dot_general | solution.py:202
  147.4 2.3 copy.27
  149.7 0.7 all-to-all-done.4
  150.3 7.8 %all-to-all-start.1 = ((bf16[2,4,128,2048]{3,2,1,0:T(8,128)(2,1)}), bf16[2,4,128,2048]{3,2,1,0:T(8,128)(2,1)}, u32[]{:S(2)}, u32[]{:S(2)}) async-start(bf16[2,4,128,2048]{3,2,1,0:T(8,128)(2,1)} %bitcast.25), calls=%async_computation.1 | async-start | bytes 8388608 | tf_op jit(solution)/shard_map/all_to_all | solution.py:91
  158.1 0.1 reduce_sum.75
  158.1 4.1 %all-to-all-done.1 = bf16[2,4,128,2048]{3,2,1,0:T(8,128)(2,1)} async-done(((bf16[2,4,128,2048]{3,2,1,0:T(8,128)(2,1)}), bf16[2,4,128,2048]{3,2,1,0:T(8,128)(2,1)}, u32[]{:S(2)}, u32[]{:S(2)}) %all-to-all-start.1) | async-done | bytes 4194336 | tf_op jit(solution)/shard_map/all_to_all | solution.py:91
  162.2 16.3 %all_to_all.40 = f32[32,1,72]{2,1,0:T(1,128)S(1)} all-to-all(f32[32,1,72]{2,1,0:T(1,128)S(1)} %broadcast_in_dim.9), channel_id=1, replica_groups=mesh['fs_0'=8,'fs_1'=4,'tp_0'=4,'tp_1'=2] {'fs_0','fs_1'}, dimensions={0} | all-to-all | bytes 18432 | tf_op jit(solution)/shard_map/all_to_all | solution.py:29
  178.5 0.7 broadcast_in_dim.11
  179.1 5.1 %all-to-all-start.6 = ((f32[8,32,72]{2,1,0:T(8,128)}), f32[8,32,72]{2,1,0:T(8,128)S(1)}, u32[]{:S(2)}, u32[]{:S(2)}) async-start(f32[8,32,72]{2,1,0:T(8,128)} %broadcast_in_dim.11), calls=%async_computation.8 | async-start | bytes 262144 | tf_op jit(solution)/shard_map/all_to_all | solution.py:29
  184.2 5.1 %reduce_sum.69 = bf16[4,128,2048]{2,1,0:T(8,128)(2,1)} reduce(bf16[2,4,128,2048]{3,2,1,0:T(8,128)(2,1)} %all-to-all-done.1, bf16[]{:T(256)} %constant.30.clone.1), dimensions={0}, to_apply=%region_0.1 | reduce | flops 1048576 | bytes 6291458 | tf_op jit(solution)/shard_map/reduce_sum | solution.py:92
  189.3 0.2 all-to-all-done.6
  189.5 4.4 %all-to-all-start.2 = ((bf16[4,128,2048]{2,1,0:T(8,128)(2,1)}), bf16[4,128,2048]{2,1,0:T(8,128)(2,1)}, u32[]{:S(2)}, u32[]{:S(2)}) async-start(bf16[4,128,2048]{2,1,0:T(8,128)(2,1)} %reduce_sum.69), calls=%async_computation.2 | async-start | bytes 4194304 | tf_op jit(solution)/shard_map/all_to_all | solution.py:99
  193.9 0.0 copy-start.7
  194.0 0.0 reduce-scatter.5.cloned.1.call-start
  194.0 0.0 reduce-scatter.3.cloned.1.call-done
  194.0 0.7 reduce-scatter.5.cloned.1.call-update
  194.7 0.0 copy-start.3
  194.7 0.0 copy-start.4
  194.7 1.3 fusion.25
  196.1 0.1 mul.155
  196.2 0.1 mul.157
  196.3 0.0 copy-done.7
  196.3 0.6 add.79
  197.0 1.4 add.80
  198.4 21.2 %all-to-all-done.2 = bf16[4,128,2048]{2,1,0:T(8,128)(2,1)} async-done(((bf16[4,128,2048]{2,1,0:T(8,128)(2,1)}), bf16[4,128,2048]{2,1,0:T(8,128)(2,1)}, u32[]{:S(2)}, u32[]{:S(2)}) %all-to-all-start.2) | async-done | bytes 2097184 | tf_op jit(solution)/shard_map/all_to_all | solution.py:99
  219.6 2.9 %reduce_sum.70 = bf16[128,2048]{1,0:T(8,128)(2,1)} reduce(bf16[4,128,2048]{2,1,0:T(8,128)(2,1)} %all-to-all-done.2, bf16[]{:T(256)} %constant.30.clone.1), dimensions={0}, to_apply=%region_1.2 | reduce | flops 786432 | bytes 2621442 | tf_op jit(solution)/shard_map/reduce_sum | solution.py:98
  222.5 0.9 convert_element_type.47
  223.4 0.0 copy-done.3
  223.4 0.0 copy-done.4
  223.4 0.7 fusion.26
  (21 shorter events, 0.2 us)
Async XLA Ops:
  7.2 2.4 %copy-start.6 = (bf16[64,384]{1,0:T(8,128)(2,1)S(1)}, bf16[64,384]{1,0:T(8,128)(2,1)}, u32[]{:S(2)}) copy-start(bf16[64,384]{1,0:T(8,128)(2,1)} %param.14) | copy-start | bytes 147460
  7.2 2.4 %copy-start.5 = (bf16[64,384]{1,0:T(8,128)(2,1)S(1)}, bf16[64,384]{1,0:T(8,128)(2,1)}, u32[]{:S(2)}) copy-start(bf16[64,384]{1,0:T(8,128)(2,1)} %param.15) | copy-start | bytes 147460
  7.2 86.7 %all-gather.2.cloned.1.call-start = ((), (), s32[]{:S(2)}) async-start(), calls=%async_computation.9 | async-start | bytes 9437184 | tf_op jit(solution)/shard_map/all_gather | solution.py:18
  11.7 82.2 %all-to-all-start = ((bf16[32,64,768]{2,1,0:T(8,128)(2,1)}), bf16[32,64,768]{2,1,0:T(8,128)(2,1)S(1)}, u32[]{:S(2)}, u32[]{:S(2)}) async-start(bf16[32,64,768]{2,1,0:T(8,128)(2,1)} %broadcast_in_dim.8), calls=%async_computation | async-start | bytes 6291456 | tf_op jit(solution)/shard_map/all_to_all | solution.py:29
  23.6 170.5 %reduce-scatter.3.cloned.1.call-start = ((), (), s32[]{:S(2)}) async-start(), calls=%async_computation.10 | async-start | bytes 3538944 | tf_op jit(solution)/shard_map/reduce_scatter | solution.py:85
  93.8 8.9 %copy-start = (bf16[32,64,768]{2,1,0:T(8,128)(2,1)}, bf16[32,64,768]{2,1,0:T(8,128)(2,1)S(1)}, u32[]{:S(2)}) copy-start(bf16[32,64,768]{2,1,0:T(8,128)(2,1)S(1)} %all-to-all-done) | copy-start | bytes 9437188
  100.2 1.1 copy-start.2
  101.3 2.2 slice-start
  102.2 2.8 %slice-start.1 = ((s8[8388608]{0:T(1024)(128)(4,1)}), s8[4194304]{0:T(1024)(128)(4,1)S(1)}, s32[]{:S(2)}) async-start(s8[8388608]{0:T(1024)(128)(4,1)} %bitcast.32), calls=%async_computation.13 | async-start | bytes 8388608
  113.3 1.2 copy-start.1
  135.5 14.8 %all-to-all-start.4 = ((f32[32,1,72]{2,1,0:T(1,128)}), f32[32,1,72]{2,1,0:T(1,128)S(1)}, u32[]{:S(2)}, u32[]{:S(2)}) async-start(f32[32,1,72]{2,1,0:T(1,128)} %bitcast.4), calls=%async_computation.6 | async-start | bytes 32768 | tf_op jit(solution)/shard_map/all_to_all | solution.py:52
  150.3 11.9 %all-to-all-start.1 = ((bf16[2,4,128,2048]{3,2,1,0:T(8,128)(2,1)}), bf16[2,4,128,2048]{3,2,1,0:T(8,128)(2,1)}, u32[]{:S(2)}, u32[]{:S(2)}) async-start(bf16[2,4,128,2048]{3,2,1,0:T(8,128)(2,1)} %bitcast.25), calls=%async_computation.1 | async-start | bytes 8388608 | tf_op jit(solution)/shard_map/all_to_all | solution.py:91
  179.1 10.3 %all-to-all-start.6 = ((f32[8,32,72]{2,1,0:T(8,128)}), f32[8,32,72]{2,1,0:T(8,128)S(1)}, u32[]{:S(2)}, u32[]{:S(2)}) async-start(f32[8,32,72]{2,1,0:T(8,128)} %broadcast_in_dim.11), calls=%async_computation.8 | async-start | bytes 262144 | tf_op jit(solution)/shard_map/all_to_all | solution.py:29
  189.5 30.1 %all-to-all-start.2 = ((bf16[4,128,2048]{2,1,0:T(8,128)(2,1)}), bf16[4,128,2048]{2,1,0:T(8,128)(2,1)}, u32[]{:S(2)}, u32[]{:S(2)}) async-start(bf16[4,128,2048]{2,1,0:T(8,128)(2,1)} %reduce_sum.69), calls=%async_computation.2 | async-start | bytes 4194304 | tf_op jit(solution)/shard_map/all_to_all | solution.py:99
  193.9 2.4 %copy-start.7 = (f32[3,3072]{1,0:T(4,128)S(1)}, f32[3,3072]{1,0:T(4,128)}, u32[]{:S(2)}) copy-start(f32[3,3072]{1,0:T(4,128)} %param.20) | copy-start | bytes 110596
  194.0 28.5 %reduce-scatter.5.cloned.1.call-start = ((), (), s32[]{:S(2)}) async-start(), calls=%async_computation.11 | async-start | bytes 491520 | tf_op jit(solution)/shard_map/reduce_scatter | solution.py:85
  194.7 28.7 %copy-start.3 = (f32[64,384]{1,0:T(8,128)S(1)}, f32[64,384]{1,0:T(8,128)}, u32[]{:S(2)}) copy-start(f32[64,384]{1,0:T(8,128)} %param.19) | copy-start | bytes 294916
  194.7 28.7 %copy-start.4 = (f32[64,384]{1,0:T(8,128)S(1)}, f32[64,384]{1,0:T(8,128)}, u32[]{:S(2)}) copy-start(f32[64,384]{1,0:T(8,128)} %param.18) | copy-start | bytes 294916
Sparse Core Ops, SparseCore 0:
  9.9 56.4 all-gather.1
  122.1 44.6 reduce-scatter.2
  197.3 17.2 reduce-scatter.4
where the time goes:
time: 231 us
  waiting for transfers between devices  96.3 us (42%)
  starting transfers between devices  35.3 us (15%)
  blocking collectives  28.7 us (12%)
  other arithmetic  23.2 us (10%)
  matrix products  23.1 us (10%)
  between operations  14.1 us (6%)
  local copies, waits for them, and re-layouts  10 us (4%)
    all_to_all x2, waiting for transfers between devices, sent_to_all(): lax.all_to_all(jnp.broadcast_to(array[None], (peers, *array.shape)), axis...  69.7 us
    all_to_all x1, waiting for transfers between devices, sum_in_two_steps(): lax.all_to_all(own.astype(jnp.bfloat16), far, 0, 0, tiled=True)  21.2 us
    all_to_all x2, starting transfers between devices, sent_to_all(): lax.all_to_all(jnp.broadcast_to(array[None], (peers, *array.shape)), axis...  16.9 us
    all_to_all x1, blocking collectives, sent_to_all(): lax.all_to_all(jnp.broadcast_to(array[None], (peers, *array.shape)), axis...  16.3 us
    all_to_all x1, blocking collectives, summed_on_arrival(): tiles = lax.all_to_all(split_up(array, dim, peers), axis, 0, 0, tiled=True)  12.4 us
    all_to_all x1, starting transfers between devices, sent_and_summed(): lax.all_to_all(tiles, axis, split_axis=0, concat_axis=0, tiled=True)  7.76 us
    dot_general x1, matrix products, make_term(): lax.dot_general(rows_all, grads, (((0,), (0,)), ((), ())), preferred_elem...  7.52 us
    dot_general x1, matrix products, shards(): jnp.dot(saved_rows, whole_weights, preferred_element_type=jnp.float32)  6.33 us
  transfers between devices with their start and end apart: 8, of which 5 were waited for; matrix products, arithmetic and copies ran while one was open for 11% of the time, Pallas kernels for 0%

commit v1 on v0

v1 whole, which is shorter than its diff:
```python
import jax
import jax.numpy as jnp
from jax import lax
from jax.experimental import pallas as pl
from jax.experimental.pallas import tpu as pltpu
from jax.sharding import Mesh
from jax.sharding import PartitionSpec as P


FS = ("z", "x")
TP = ("y", "c")
FS_TP = ("z", "x", "y", "c")
BF16 = jnp.bfloat16
F32 = jnp.float32
LANES = 128
CHUNK = 64
KERNEL_VMEM = 20 << 20


def shift(array, axis, steps):
    peers = lax.axis_size(axis)
    return lax.ppermute(array, axis, [(i, (i + steps) % peers) for i in range(peers)])


def swapped(array, axis):
    return lax.ppermute(array, axis, [(0, 1), (1, 0)])


def exchanged(tiles, axis):
    return lax.all_to_all(tiles, axis, 0, 0, tiled=True)


def from_all(array, axis):
    return exchanged(jnp.broadcast_to(array[None], (lax.axis_size(axis), *array.shape)), axis)


def tiles_kernel(up_ref, gate_ref, tiles_ref):
    cols = up_ref.shape[1]
    for peer in range(tiles_ref.shape[0]):
        tiles_ref[peer, :, :cols] = up_ref[...]
        tiles_ref[peer, :, cols:] = gate_ref[...]


def rows_kernel(saved_ref, later_ref, rows_ref):
    rows_ref[0] = saved_ref[...]
    rows_ref[1] = later_ref[...]


def packed(kernel, shape, *arrays):
    return pl.pallas_call(
        kernel,
        out_shape=jax.ShapeDtypeStruct(shape, BF16),
        compiler_params=pltpu.CompilerParams(vmem_limit_bytes=8 << 20),
    )(*arrays)


def gather_rows(rows):
    y = lax.axis_index("y")
    half = rows.shape[1] // 2
    from_low = shift(rows, "y", 1)
    from_high = shift(rows, "y", -1)
    far_top = shift(from_low[:, :half], "y", 1)
    far_low = shift(from_high[:, half:], "y", -1)

    def placed(i):
        own = jnp.zeros((4, *rows.shape[1:]), rows.dtype)

        def put_rows(whole, block, index, start=0):
            return lax.dynamic_update_slice(whole, block[i][None], (index % 4, start, 0))

        own = put_rows(own, rows, y)
        own = put_rows(own, from_low, y + 3)
        own = put_rows(own, from_high, y + 1)
        own = put_rows(own, far_top, y + 2)
        own = put_rows(own, far_low, y + 2, half)
        return own.reshape(-1, rows.shape[2])

    saved, later = placed(0), placed(1)
    return (saved, swapped(saved, "c")), (later, swapped(later, "c"))


def project_into(own_ref, other_ref, up_ref, gate_ref, core_ref, values_ref):
    values_ref[:8, :] = jnp.zeros((8, values_ref.shape[1]), F32)
    weight = jnp.concatenate([up_ref[...], gate_ref[...]], axis=1)
    block = own_ref.shape[0] // 4
    for rows_ref, core in ((own_ref, core_ref[0]), (other_ref, 1 - core_ref[0])):
        part = jnp.dot(rows_ref[...], weight, preferred_element_type=F32)
        part = part.astype(BF16).astype(F32)
        for y in range(4):
            at = pl.multiple_of(8 + y * 2 * block + core * block, 8)
            values_ref[pl.ds(at, block), :] = part[y * block : (y + 1) * block]


def convolved(values, taps_ref):
    one, two, zero = pltpu.roll(values, 1, 0)[8:], pltpu.roll(values, 2, 0)[8:], values[8:]
    out = taps_ref[2:3, :] * zero + taps_ref[1:2, :] * one + taps_ref[0:1, :] * two
    return [two, one, zero], out


def hidden_kernel(
    core_ref, own_ref, other_ref, up_ref, gate_ref, taps_up_ref, taps_gate_ref, hidden_ref, values_ref
):
    project_into(own_ref, other_ref, up_ref, gate_ref, core_ref, values_ref)

    def step(i, carry):
        at = pl.multiple_of(i * CHUNK, CHUNK)
        up = convolved(values_ref[pl.ds(at, CHUNK + 8), :LANES], taps_up_ref)[1]
        gate = convolved(values_ref[pl.ds(at, CHUNK + 8), LANES:], taps_gate_ref)[1]
        hidden_ref[pl.ds(at, CHUNK), :] = (gate / (1.0 + jnp.exp(-gate)) * up).astype(BF16)
        return carry

    lax.fori_loop(0, hidden_ref.shape[0] // CHUNK, step, 0)


def grads_kernel(
    core_ref,
    own_ref,
    other_ref,
    up_ref,
    gate_ref,
    taps_up_ref,
    taps_gate_ref,
    cotangent_ref,
    grads_ref,
    sums_ref,
    values_ref,
    conv_ref,
):
    project_into(own_ref, other_ref, up_ref, gate_ref, core_ref, values_ref)
    tokens = 2 * own_ref.shape[0]
    count = tokens // CHUNK
    conv_ref[pl.ds(tokens, 8), :] = jnp.zeros((8, conv_ref.shape[1]), F32)
    lanes = [
        pl.ds(pl.multiple_of(pl.program_id(0) * LANES + part * (grads_ref.shape[1] // 2), LANES), LANES)
        for part in range(2)
    ]

    def step(i, sums):
        at = pl.multiple_of(i * CHUNK, CHUNK)
        ups, up = convolved(values_ref[pl.ds(at, CHUNK + 8), :LANES], taps_up_ref)
        gates, gate = convolved(
            values_ref[pl.ds(at, CHUNK + 8), LANES:], taps_gate_ref
        )
        sig = 1.0 / (1.0 + jnp.exp(-gate))
        upstream = cotangent_ref[pl.ds(at, CHUNK), :].astype(F32)
        grad_up = upstream * (gate * sig)
        grad_gate = upstream * up * sig * (1.0 + gate * (1.0 - sig))
        conv_ref[pl.ds(at, CHUNK), :LANES] = grad_up
        conv_ref[pl.ds(at, CHUNK), LANES:] = grad_gate

        def folded(values):
            return jnp.sum(values.reshape(CHUNK // 8, 8, LANES), axis=0)

        new = [folded(grad_up * v) for v in ups] + [folded(grad_gate * v) for v in gates]
        return tuple(a + b for a, b in zip(sums, new))

    zero = jnp.zeros((8, LANES), F32)
    sums = lax.fori_loop(0, count, step, (zero,) * 6)
    for k in range(3):
        for part in range(2):
            sums_ref[k : k + 1, lanes[part]] = jnp.sum(
                sums[3 * part + k], axis=0, keepdims=True
            )

    block = tokens // 8
    per_block = block // CHUNK

    def back(i, carry):
        at = pl.multiple_of(i * CHUNK, CHUNK)
        size = CHUNK + 8
        b = i // per_block
        away = lax.rem(b + core_ref[0], 2)
        to = away * (4 * block) + (b // 2) * block + lax.rem(i, per_block) * CHUNK
        to = pl.ds(pl.multiple_of(to, CHUNK), CHUNK)
        for part, taps_ref in enumerate((taps_up_ref, taps_gate_ref)):
            g = conv_ref[pl.ds(at, size), part * LANES : (part + 1) * LANES]
            one = pltpu.roll(g, size - 1, 0)[:CHUNK]
            two = pltpu.roll(g, size - 2, 0)[:CHUNK]
            out = taps_ref[2:3, :] * g[:CHUNK] + taps_ref[1:2, :] * one + taps_ref[0:1, :] * two
            grads_ref[to, lanes[part]] = out.astype(BF16)
        return carry

    lax.fori_loop(0, count, back, 0)


def common_specs(weights):
    steps = weights.shape[1] // (2 * LANES)
    whole = pl.BlockSpec(memory_space=pltpu.VMEM)
    taps = pl.BlockSpec((3, LANES), lambda j: (0, j))
    return [
        pl.BlockSpec(memory_space=pltpu.SMEM),
        whole,
        whole,
        pl.BlockSpec((weights.shape[0], LANES), lambda j: (0, j)),
        pl.BlockSpec((weights.shape[0], LANES), lambda j: (0, j + steps)),
        taps,
        taps,
    ]


def hidden_of(core, own, other, weights, taps_up, taps_gate):
    tokens, steps = 2 * own.shape[0], weights.shape[1] // (2 * LANES)
    return pl.pallas_call(
        hidden_kernel,
        grid=(steps,),
        in_specs=common_specs(weights),
        out_specs=pl.BlockSpec((tokens, LANES), lambda j: (0, j)),
        out_shape=jax.ShapeDtypeStruct((tokens, steps * LANES), BF16),
        scratch_shapes=[pltpu.VMEM((tokens + 8, 2 * LANES), F32)],
        compiler_params=pltpu.CompilerParams(vmem_limit_bytes=KERNEL_VMEM),
        cost_estimate=pl.CostEstimate(
            flops=2 * tokens * weights.size, transcendentals=0, bytes_accessed=8 << 20
        ),
    )(core, own, other, weights, weights, taps_up, taps_gate)


def grads_of(core, own, other, weights, taps_up, taps_gate, cotangent):
    tokens, steps = 2 * own.shape[0], weights.shape[1] // (2 * LANES)
    return pl.pallas_call(
        grads_kernel,
        grid=(steps,),
        in_specs=common_specs(weights)
        + [pl.BlockSpec((tokens, LANES), lambda j: (0, j))],
        out_specs=[
            pl.BlockSpec((tokens, weights.shape[1]), lambda j: (0, 0)),
            pl.BlockSpec((3, weights.shape[1]), lambda j: (0, 0)),
        ],
        out_shape=[
            jax.ShapeDtypeStruct((tokens, weights.shape[1]), BF16),
            jax.ShapeDtypeStruct((3, weights.shape[1]), F32),
        ],
        scratch_shapes=[
            pltpu.VMEM((tokens + 8, 2 * LANES), F32),
            pltpu.VMEM((tokens + 8, 2 * LANES), F32),
        ],
        compiler_params=pltpu.CompilerParams(vmem_limit_bytes=KERNEL_VMEM),
        cost_estimate=pl.CostEstimate(
            flops=2 * tokens * weights.size, transcendentals=0, bytes_accessed=8 << 20
        ),
    )(core, own, other, weights, weights, taps_up, taps_gate, cotangent)


def sum_rows_to_owner(grads, weights):
    half = grads.shape[0] // 2

    def partial(rows):
        out = lax.dot_general(rows, weights, (((1,), (1,)), ((), ())), preferred_element_type=F32)
        return out.astype(BF16)

    arrived = swapped(partial(grads[half:]), "c")
    chunks = (partial(grads[:half]).astype(F32) + arrived.astype(F32)).astype(BF16)
    y = lax.axis_index("y")
    chunks = chunks.reshape(4, -1, chunks.shape[1])
    half = chunks.shape[1] // 2

    def take(step):
        return lax.dynamic_index_in_dim(chunks, (y + step) % 4, 0, keepdims=False)

    far = take(2)
    far_top = shift(far[:half], "y", 1).astype(F32)
    far_low = shift(far[half:], "y", -1).astype(F32)
    up, down = take(1).astype(F32), take(3).astype(F32)
    up = jnp.concatenate([up[:half] + far_top, up[half:]], axis=0).astype(BF16)
    down = jnp.concatenate([down[:half], down[half:] + far_low], axis=0).astype(BF16)
    from_low = shift(up, "y", 1).astype(F32)
    from_high = shift(down, "y", -1).astype(F32)
    return (take(0).astype(F32) + from_low + from_high).astype(BF16)


def sum_to_owner_x(block):
    tiles = block.reshape(4, -1, block.shape[1])
    return exchanged(tiles, "x").astype(F32).sum(axis=0)


def body(
    later_input,
    saved_input,
    cotangent,
    up_weight,
    gate_weight,
    up_taps,
    gate_taps,
    up_grad_sum,
    gate_grad_sum,
    up_taps_sum,
    gate_taps_sum,
):
    cols = up_weight.shape[1]
    group = lax.axis_size(TP)
    offset = lax.axis_index(TP) * cols
    tokens = later_input.shape[0] * lax.axis_size(FS) * group
    grad_scale = jnp.float32(tokens ** (-0.5))
    taps_up = lax.dynamic_slice_in_dim(up_taps, offset, cols, 1).astype(F32)
    taps_gate = lax.dynamic_slice_in_dim(gate_taps, offset, cols, 1).astype(F32)
    core = jnp.full((1,), lax.axis_index("c"), jnp.int32)

    tiles = packed(tiles_kernel, (4, up_weight.shape[0], 2 * cols), up_weight, gate_weight)
    rows = packed(rows_kernel, (2, *saved_input.shape), saved_input, later_input)
    near = exchanged(tiles, "x").reshape(-1, 2 * cols)
    weights = lax.all_gather(near, "z", axis=0, tiled=True)
    saved, later = gather_rows(rows)

    both = jnp.concatenate(saved, axis=0)
    both, saved, later = lax.optimization_barrier((both, saved, later))
    grads, taps_local = grads_of(core, *saved, weights, taps_up, taps_gate, cotangent)
    term = lax.dot_general(
        both, grads, (((0,), (0,)), ((), ())), preferred_element_type=F32
    ).astype(BF16)
    own_z = lax.psum_scatter(term, "z", scatter_dimension=0, tiled=True)

    input_grad = sum_rows_to_owner(grads, weights)
    hidden = hidden_of(core, *later, weights, taps_up, taps_gate)
    taps_z = from_all(taps_local, "z").sum(axis=0)
    taps_all = from_all(from_all(taps_z, TP), "x").sum(axis=0)

    own = sum_to_owner_x(own_z)
    taps_all = taps_all.reshape(group, 3, 2, cols).transpose(2, 1, 0, 3).reshape(2, 3, -1)
    return (
        hidden,
        input_grad,
        up_grad_sum + grad_scale * own[:, :cols],
        gate_grad_sum + grad_scale * own[:, cols:],
        up_taps_sum + grad_scale * taps_all[0],
        gate_taps_sum + grad_scale * taps_all[1],
    )


def solution(mesh):
    finer = Mesh(mesh.devices.reshape(8, 4, 4, 2), ("z", "x", "y", "c"))
    in_specs = (
        P(FS_TP, None),
        P(FS_TP, None),
        P(FS, TP),
        P(FS, TP),
        P(FS, TP),
        P(),
        P(),
        P(FS, TP),
        P(FS, TP),
        P(),
        P(),
    )
    out_specs = (P(FS, TP), P(FS_TP, None), P(FS, TP), P(FS, TP), P(), P())
    return jax.shard_map(body, mesh=finer, in_specs=in_specs, out_specs=out_specs, check_vma=False)
```

time: 231 us -> 178 us (0.77)
  waiting for transfers between devices: 96.3 us -> 38.3 us
  Pallas kernels: 0 us -> 19.9 us
  local copies, waits for them, and re-layouts: 10 us -> 23 us
  matrix products: 23.1 us -> 12.8 us
  other arithmetic: 23.2 us -> 13.5 us
  blocking collectives: 28.7 us -> 23.5 us
  starting transfers between devices: 35.3 us -> 30.8 us
    all_to_all x5 -> x3, waiting for transfers between devices: 95.6 us -> 8.11 us  [exchanged(): return lax.all_to_all(tiles, axis, 0, 0, tiled=True)]
    ppermute x0 -> x11, waiting for transfers between devices: none -> 30.2 us  [the longest x8 22.8 us: shift(): lax.ppermute(array, axis, [(i, (i + steps) % peers) for i in range(peers)])]
    pallas_call x0 -> x4, Pallas kernels: none -> 19.9 us  [the longest x1 10.4 us: grads_of(): pl.pallas_call(grads_kernel, grid=(steps,), in_specs=common_specs(weights...]
    all_to_all x5 -> x3, starting transfers between devices: 35.1 us -> 15.7 us  [exchanged(): return lax.all_to_all(tiles, axis, 0, 0, tiled=True)]
    ppermute x0 -> x11, starting transfers between devices: none -> 15 us  [the longest x8 11.3 us: shift(): lax.ppermute(array, axis, [(i, (i + steps) % peers) for i in range(peers)])]
    reduce_sum x5 -> x3, other arithmetic: 13.5 us -> 0.1 us  [the longest x1 0.05 us: sum_to_owner_x(): return exchanged(tiles, 'x').astype(F32).sum(axis=0)]
    dot_general x4 -> x3, matrix products: 23.1 us -> 12.8 us  [the longest x2 7.96 us: partial(): lax.dot_general(rows, weights, (((1,), (1,)), ((), ())), preferred_elemen...]
    dynamic_update_slice x2 -> x6, local copies, waits for them, and re-layouts: 0.03 us -> 6.65 us  [put_rows(): lax.dynamic_update_slice(whole, block[i][None], (index % 4, start, 0))]
  transfers between devices with their start and end apart: 8 -> 16, of which waited for: 5 -> 6; matrix products, arithmetic and copies ran while one was open for 11% -> 19% of each run, Pallas kernels for 0% -> 5%
where the time goes in v1:
time: 178 us; the launch traced here: 176 us
  waiting for transfers between devices  38.3 us (22%)
  starting transfers between devices  30.8 us (17%)
  blocking collectives  23.5 us (13%)
  local copies, waits for them, and re-layouts  23 us (13%)
  Pallas kernels  19.9 us (11%)
  between operations  14.3 us (8%)
  other arithmetic  13.5 us (8%)
  matrix products  12.8 us (7%)
    all_to_all x2, blocking collectives, exchanged(): return lax.all_to_all(tiles, axis, 0, 0, tiled=True)  23.5 us
    ppermute x8, waiting for transfers between devices, shift(): lax.ppermute(array, axis, [(i, (i + steps) % peers) for i in range(peers)])  22.8 us
    all_to_all x3, starting transfers between devices, exchanged(): return lax.all_to_all(tiles, axis, 0, 0, tiled=True)  15.7 us
    ppermute x8, starting transfers between devices, shift(): lax.ppermute(array, axis, [(i, (i + steps) % peers) for i in range(peers)])  11.3 us
    pallas_call x1, Pallas kernels, grads_of(): pl.pallas_call(grads_kernel, grid=(steps,), in_specs=common_specs(weights...  10.4 us
    unnamed x30, local copies, waits for them, and re-layouts  9.96 us
    pallas_call x1, Pallas kernels, hidden_of(): pl.pallas_call(hidden_kernel, grid=(steps,), in_specs=common_specs(weight...  9.38 us
    all_to_all x3, waiting for transfers between devices, exchanged(): return lax.all_to_all(tiles, axis, 0, 0, tiled=True)  8.11 us
  transfers between devices with their start and end apart: 16, of which 6 were waited for; matrix products, arithmetic and copies ran while one was open for 19% of the time, Pallas kernels for 5%

profile of v1, /device:TPU:1, one launch (start us, length us, event | category | flops | bytes accessed | tf_op | source)
XLA Modules:
  0.0 176.2 jit_solution(16622292728585396582)
XLA Ops:
  7.2 0.0 all-gather.2.cloned.1.call-start
  7.2 0.8 copy-done.2
  8.0 0.8 copy-done.3
  8.8 11.1 %all_to_all.25 = bf16[4,64,768]{2,1,0:T(8,128)(2,1)} all-to-all(bf16[4,64,768]{2,1,0:T(8,128)(2,1)S(1)} %shard_map.155), channel_id=1, replica_groups=mesh['z'=8,'x'=4,'y'=4,'c'=2] {'x'}, dimensions={0} | all-to-all | bytes 786432 | tf_op jit(solution)/shard_map/all_to_all | solution.py:30
  19.9 0.0 all-gather.2.cloned.1.call-update
  20.0 0.0 reduce-scatter.2.cloned.1.call-start
  20.0 1.0 copy-done
  21.0 1.0 copy-done.1
  22.1 0.1 shard_map.154
  22.2 2.3 %collective-permute-start = (bf16[2,128,2048]{2,1,0:T(8,128)(2,1)S(1)}, bf16[2,128,2048]{2,1,0:T(8,128)(2,1)}, u32[]{:S(2)}, u32[]{:S(2)}) collective-permute-start(bf16[2,128,2048]{2,1,0:T(8,128)(2,1)S(1)} %shard_map.154), channel_id=1, source_target_pairs={{0,2},{2,4},{4,6},{6,0},{1,3},{3,5},{5,7},{7,1},{8,10},{10,12},{12... | collective-permute-start | bytes 3145736 | tf_op jit(solution)/shard_map/ppermute | solution.py:22
  24.4 1.5 collective-permute-start.1
  25.9 1.7 broadcast.19.clone
  27.6 0.8 slice_dynamic-update-slice_fusion.2
  28.4 0.2 broadcast.19.clone.1
  28.7 0.1 slice_dynamic-update-slice_fusion.5
  28.8 18.7 %collective-permute-done = bf16[2,128,2048]{2,1,0:T(8,128)(2,1)} collective-permute-done((bf16[2,128,2048]{2,1,0:T(8,128)(2,1)S(1)}, bf16[2,128,2048]{2,1,0:T(8,128)(2,1)}, u32[]{:S(2)}, u32[]{:S(2)}) %collective-permute-start) | collective-permute-done | bytes 1048608 | tf_op jit(solution)/shard_map/ppermute | solution.py:22
  47.5 1.1 slice.137
  48.5 0.1 collective-permute-start.2
  48.6 1.1 slice.139
  49.7 2.7 %collective-permute-start.3 = (bf16[2,64,2048]{2,1,0:T(8,128)(2,1)S(1)}, bf16[2,64,2048]{2,1,0:T(8,128)(2,1)S(1)}, u32[]{:S(2)}, u32[]{:S(2)}) collective-permute-start(bf16[2,64,2048]{2,1,0:T(8,128)(2,1)S(1)} %slice.139), channel_id=1, source_target_pairs={{0,6},{2,0},{4,2},{6,4},{1,7},{3,1},{5,3},{7,5},{8,14},{10,8},{12,... | collective-permute-start | bytes 1572872 | tf_op jit(solution)/shard_map/ppermute | solution.py:22
  52.5 2.1 %slice_dynamic-update-slice_fusion.1 = (bf16[4,128,2048]{2,1,0:T(8,128)(2,1)}, bf16[4,128,2048]{2,1,0:T(8,128)(2,1)S(1)}) fusion(bf16[4,128,2048]{2,1,0:T(8,128)(2,1)} %slice_dynamic-update-slice_fusion.2, s32[]{:T(128)S(6)} %select_n.69, bf16[2,128,2048]{2,1,0:T(8,128)(2,1)} %collective-permute-done, ...), kind=kLoop, calls=%fused_computation.12 | loop fusion | bytes 2097156 | tf_op jit(solution)/shard_map/dynamic_update_slice | solution.py:69
  54.6 2.1 %slice_dynamic-update-slice_fusion = (bf16[4,128,2048]{2,1,0:T(8,128)(2,1)}, bf16[4,128,2048]{2,1,0:T(8,128)(2,1)S(1)}) fusion(bf16[4,128,2048]{2,1,0:T(8,128)(2,1)} %get-tuple-element.30, s32[]{:T(128)S(6)} %select_n.71, bf16[2,128,2048]{2,1,0:T(8,128)(2,1)} %collective-permute-done.1, bf16[4,128,2048]{2,1,0:T(8,128)(2,1)S(1)} %get-tuple-element.31), kind=kLoop, calls=%fused_computation.11 | loop fusion | bytes 2097156 | tf_op jit(solution)/shard_map/dynamic_update_slice | solution.py:69
  56.7 4.1 %collective-permute-done.2 = bf16[2,64,2048]{2,1,0:T(8,128)(2,1)S(1)} collective-permute-done((bf16[2,64,2048]{2,1,0:T(8,128)(2,1)S(1)}, bf16[2,64,2048]{2,1,0:T(8,128)(2,1)S(1)}, u32[]{:S(2)}, u32[]{:S(2)}) %collective-permute-start.2) | collective-permute-done | bytes 524320 | tf_op jit(solution)/shard_map/ppermute | solution.py:22
  60.8 0.8 slice_dynamic-update-slice_fusion.7
  61.6 0.7 slice_dynamic-update-slice_fusion.6
  62.3 3.4 %collective-permute-start.4 = (bf16[512,2048]{1,0:T(8,128)(2,1)S(1)}, bf16[512,2048]{1,0:T(8,128)(2,1)}, u32[]{:S(2)}, u32[]{:S(2)}) collective-permute-start(bf16[512,2048]{1,0:T(8,128)(2,1)S(1)} %bitcast.38), channel_id=1, source_target_pairs={{0,1},{1,0},{2,3},{3,2},{4,5},{5,4},{6,7},{7,6},{8,9},{9,8},{10,11... | collective-permute-start | bytes 6291464 | tf_op jit(solution)/shard_map/ppermute | solution.py:26
  65.7 0.7 fusion.10
  66.4 3.2 %collective-permute-done.4.other_ref = bf16[512,2048]{1,0:T(8,128)(2,1)} collective-permute-done((bf16[512,2048]{1,0:T(8,128)(2,1)S(1)}, bf16[512,2048]{1,0:T(8,128)(2,1)}, u32[]{:S(2)}, u32[]{:S(2)}) %collective-permute-start.4) | collective-permute-done | bytes 2097184 | tf_op jit(solution)/shard_map/ppermute | solution.py:26
  69.6 4.1 %pad_maximum_fusion = bf16[1024,2048]{1,0:T(8,128)(2,1)} fusion(bf16[512,2048]{1,0:T(8,128)(2,1)} %collective-permute-done.4.other_ref, bf16[512,2048]{1,0:T(8,128)(2,1)S(1)} %bitcast.39), kind=kLoop, calls=%fused_computation | loop fusion | flops 8388608 | bytes 8388608 | tf_op jit(solution)/shard_map/concatenate | solution.py:303
  73.7 1.9 %copy-done.4 = bf16[2048,768]{1,0:T(8,128)(2,1)S(1)} copy-done((bf16[2048,768]{1,0:T(8,128)(2,1)S(1)}, bf16[2048,768]{1,0:T(8,128)(2,1)}, u32[]{:S(2)}) %copy-start.4) | copy-done | bytes 3145752
  75.6 10.4 %shard_map.157 = (bf16[1024,768]{1,0:T(8,128)(2,1)S(1)}, f32[3,768]{1,0:T(4,128)S(1)}) custom-call(s32[1]{0:T(128)} %bitcast.core_ref, bf16[512,2048]{1,0:T(8,128)(2,1)S(1)} %bitcast.40, bf16[512,2048]{1,0:T(8,128)(2,1)} %collective-permute-done.4.other_ref, bf16[2048,768]{1,0:T(8,128)(2,1)S(1)} %copy-done.4, bf16[2048,768]{1,0:T(8,128)(2,1)S(1)} %copy-done.4, ...), custom_call_target="tpu_custom_call" | custom-call | flops 3221225472 | bytes 8388608 | tf_op jit(solution)/shard_map/pallas_call | solution.py:219
  86.0 1.1 copy-done.7
  87.2 4.9 %convolution_convert_fusion = bf16[2048,768]{1,0:T(8,128)(2,1)} fusion(bf16[1024,2048]{1,0:T(8,128)(2,1)S(1)} %copy-done.8, bf16[1024,768]{1,0:T(8,128)(2,1)S(1)} %get-tuple-element.17), kind=kOutput, calls=%fused_computation.2 | convolution fusion | flops 3222798336 | bytes 8912896 | tf_op jit(solution)/shard_map/dot_general | solution.py:306
  92.1 0.0 reduce-scatter.2.cloned.1.call-update
  92.1 1.9 %copy-done.5 = bf16[2048,768]{1,0:T(8,128)(2,1)S(1)} copy-done((bf16[2048,768]{1,0:T(8,128)(2,1)S(1)}, bf16[2048,768]{1,0:T(8,128)(2,1)}, u32[]{:S(2)}) %copy-start.5) | copy-done | bytes 3145752
  93.9 4.3 %convolution_convert_fusion.1 = bf16[512,2048]{1,0:T(8,128)(2,1)} fusion(bf16[2048,768]{1,0:T(8,128)(2,1)S(1)} %copy-done.5, bf16[1024,768]{1,0:T(8,128)(2,1)} %copy-done.7), kind=kOutput, calls=%fused_computation.3 | convolution fusion | flops 1611661312 | bytes 6029312 | tf_op jit(solution)/shard_map/dot_general | solution.py:247
  98.2 0.4 collective-permute-start.6
  98.6 4.1 %collective-permute-done.6 = bf16[512,2048]{1,0:T(8,128)(2,1)} collective-permute-done((bf16[512,2048]{1,0:T(8,128)(2,1)}, bf16[512,2048]{1,0:T(8,128)(2,1)}, u32[]{:S(2)}, u32[]{:S(2)}) %collective-permute-start.6) | collective-permute-done | bytes 2097184 | tf_op jit(solution)/shard_map/ppermute | solution.py:26
  102.7 3.7 %add_convert_fusion = bf16[512,2048]{1,0:T(8,128)(2,1)S(1)} fusion(bf16[512,2048]{1,0:T(8,128)(2,1)} %collective-permute-done.6, bf16[2048,768]{1,0:T(8,128)(2,1)S(1)} %copy-done.5, bf16[1024,768]{1,0:T(8,128)(2,1)} %copy-done.7), kind=kOutput, calls=%fused_computation.1 | convolution fusion | flops 1615855616 | bytes 8126464 | tf_op jit(solution)/shard_map/dot_general | solution.py:247
  106.4 1.3 copy-done.9
  107.8 0.9 dynamic-slice_bitcast_fusion.4
  108.7 0.4 collective-permute-start.7
  109.1 2.8 %collective-permute-start.9 = (bf16[64,2048]{1,0:T(8,128)(2,1)}, bf16[64,2048]{1,0:T(8,128)(2,1)}, u32[]{:S(2)}, u32[]{:S(2)}) collective-permute-start(bf16[64,2048]{1,0:T(8,128)(2,1)} %get-tuple-element.26), channel_id=1, source_target_pairs={{0,6},{2,0},{4,2},{6,4},{1,7},{3,1},{5,3},{7,5},{8,14},{10,8},{12,... | collective-permute-start | bytes 786440 | tf_op jit(solution)/shard_map/ppermute | solution.py:22
  111.9 0.7 broadcast_in_dim.9
  112.5 8.1 %all-to-all-start.2 = ((f32[8,3,768]{2,1,0:T(4,128)}), f32[8,3,768]{2,1,0:T(4,128)S(1)}, u32[]{:S(2)}, u32[]{:S(2)}) async-start(f32[8,3,768]{2,1,0:T(4,128)} %broadcast_in_dim.9), calls=%async_computation.3 | async-start | bytes 196608 | tf_op jit(solution)/shard_map/all_to_all | solution.py:30
  120.7 1.3 fusion.5
  122.0 1.8 %pad_maximum_fusion.2 = bf16[128,2048]{1,0:T(8,128)(2,1)} fusion(bf16[64,2048]{1,0:T(8,128)(2,1)S(1)} %get-tuple-element.23, bf16[64,2048]{1,0:T(8,128)(2,1)} %get-tuple-element.25), kind=kLoop, calls=%fused_computation.18 | loop fusion | flops 1048576 | bytes 1048576 | tf_op jit(solution)/shard_map/concatenate | solution.py:264
  123.8 1.5 collective-permute-start.10
  125.3 0.8 pad_maximum_fusion.1
  126.1 3.8 %all-to-all-done.2 = f32[8,3,768]{2,1,0:T(4,128)S(1)} async-done(((f32[8,3,768]{2,1,0:T(4,128)}), f32[8,3,768]{2,1,0:T(4,128)S(1)}, u32[]{:S(2)}, u32[]{:S(2)}) %all-to-all-start.2) | async-done | bytes 73760 | tf_op jit(solution)/shard_map/all_to_all | solution.py:30
  129.9 12.5 %all_to_all.26 = f32[8,3,768]{2,1,0:T(4,128)S(1)} all-to-all(f32[8,3,768]{2,1,0:T(4,128)S(1)} %broadcast_in_dim.10), channel_id=1, replica_groups=mesh['z'=8,'x'=4,'y'=4,'c'=2] {'y','c'}, dimensions={0} | all-to-all | bytes 147456 | tf_op jit(solution)/shard_map/all_to_all | solution.py:30
  142.4 0.7 broadcast_in_dim.11
  143.1 3.5 %all-to-all-start.4 = ((f32[4,8,3,768]{3,1,2,0:T(8,128)}), f32[4,8,3,768]{3,1,2,0:T(8,128)S(1)}, u32[]{:S(2)}, u32[]{:S(2)}) async-start(f32[4,8,3,768]{3,1,2,0:T(8,128)} %broadcast_in_dim.11), calls=%async_computation.5 | async-start | bytes 589824 | tf_op jit(solution)/shard_map/all_to_all | solution.py:30
  146.6 0.0 copy-start.12
  146.6 0.0 copy-start.13
  146.6 9.4 %shard_map.156 = bf16[1024,384]{1,0:T(8,128)(2,1)} custom-call(s32[1]{0:T(128)} %bitcast.core_ref, bf16[512,2048]{1,0:T(8,128)(2,1)} %bitcast.2.own_ref, bf16[512,2048]{1,0:T(8,128)(2,1)} %collective-permute-done.5.other_ref, bf16[2048,768]{1,0:T(8,128)(2,1)S(1)} %copy-done.5, bf16[2048,768]{1,0:T(8,128)(2,1)S(1)} %copy-done.5, ...), custom_call_target="tpu_custom_call" | custom-call | flops 3221225472 | bytes 8388608 | tf_op jit(solution)/shard_map/pallas_call | solution.py:203
  156.1 0.2 fusion.8
  156.4 0.6 add.119
  157.0 0.6 add.120
  157.6 4.2 %all-to-all-start.1 = ((bf16[4,64,768]{2,1,0:T(8,128)(2,1)}), bf16[4,64,768]{2,1,0:T(8,128)(2,1)S(1)}, u32[]{:S(2)}, u32[]{:S(2)}) async-start(bf16[4,64,768]{2,1,0:T(8,128)(2,1)} %bitcast.45), calls=%async_computation.2 | async-start | bytes 786432 | tf_op jit(solution)/shard_map/all_to_all | solution.py:30
  161.8 2.4 %fusion.1 = bf16[128,2048]{1,0:T(8,128)(2,1)} fusion(bf16[128,2048]{1,0:T(8,128)(2,1)} %collective-permute-done.10, bf16[128,2048]{1,0:T(8,128)(2,1)} %collective-permute-done.8, bf16[4,128,2048]{2,1,0:T(8,128)(2,1)} %bitcast.43, s32[]{:T(128)S(6)} %select_n.67), kind=kLoop, calls=%fused_computation.7 | loop fusion | flops 1572864 | bytes 2097156 | tf_op jit(solution)/shard_map/convert_element_type | solution.py:267
  164.2 4.4 %all-to-all-done.1 = bf16[4,64,768]{2,1,0:T(8,128)(2,1)S(1)} async-done(((bf16[4,64,768]{2,1,0:T(8,128)(2,1)}), bf16[4,64,768]{2,1,0:T(8,128)(2,1)S(1)}, u32[]{:S(2)}, u32[]{:S(2)}) %all-to-all-start.1) | async-done | bytes 393248 | tf_op jit(solution)/shard_map/all_to_all | solution.py:30
  168.6 0.1 convert_reduce_fusion
  168.6 0.7 fusion.6
  (38 shorter events, 0.3 us)
Async XLA Ops:
  7.2 66.5 %all-gather.2.cloned.1.call-start = ((), (), s32[]{:S(2)}) async-start(), calls=%async_computation.6 | async-start | bytes 3538944 | tf_op jit(solution)/shard_map/all_gather | solution.py:300
  7.2 0.8 copy-start.2
  8.0 0.8 copy-start.3
  20.0 137.7 %reduce-scatter.2.cloned.1.call-start = ((), (), s32[]{:S(2)}) async-start(), calls=%async_computation.7 | async-start | bytes 3538944 | tf_op jit(solution)/shard_map/reduce_scatter | solution.py:309
  20.0 1.0 copy-start
  21.0 1.0 copy-start.1
  22.2 25.3 %collective-permute-start = (bf16[2,128,2048]{2,1,0:T(8,128)(2,1)S(1)}, bf16[2,128,2048]{2,1,0:T(8,128)(2,1)}, u32[]{:S(2)}, u32[]{:S(2)}) collective-permute-start(bf16[2,128,2048]{2,1,0:T(8,128)(2,1)S(1)} %shard_map.154), channel_id=1, source_target_pairs={{0,2},{2,4},{4,6},{6,0},{1,3},{3,5},{5,7},{7,1},{8,10},{10,12},{12... | collective-permute-start | bytes 3145736 | tf_op jit(solution)/shard_map/ppermute | solution.py:22
  24.4 24.2 %collective-permute-start.1 = (bf16[2,128,2048]{2,1,0:T(8,128)(2,1)S(1)}, bf16[2,128,2048]{2,1,0:T(8,128)(2,1)}, u32[]{:S(2)}, u32[]{:S(2)}) collective-permute-start(bf16[2,128,2048]{2,1,0:T(8,128)(2,1)S(1)} %shard_map.154), channel_id=1, source_target_pairs={{0,6},{2,0},{4,2},{6,4},{1,7},{3,1},{5,3},{7,5},{8,14},{10,8},{12,... | collective-permute-start | bytes 3145736 | tf_op jit(solution)/shard_map/ppermute | solution.py:22
  48.5 12.3 %collective-permute-start.2 = (bf16[2,64,2048]{2,1,0:T(8,128)(2,1)S(1)}, bf16[2,64,2048]{2,1,0:T(8,128)(2,1)S(1)}, u32[]{:S(2)}, u32[]{:S(2)}) collective-permute-start(bf16[2,64,2048]{2,1,0:T(8,128)(2,1)S(1)} %slice.137), channel_id=1, source_target_pairs={{0,2},{2,4},{4,6},{6,0},{1,3},{3,5},{5,7},{7,1},{8,10},{10,12},{12... | collective-permute-start | bytes 1572872 | tf_op jit(solution)/shard_map/ppermute | solution.py:22
  49.7 11.8 %collective-permute-start.3 = (bf16[2,64,2048]{2,1,0:T(8,128)(2,1)S(1)}, bf16[2,64,2048]{2,1,0:T(8,128)(2,1)S(1)}, u32[]{:S(2)}, u32[]{:S(2)}) collective-permute-start(bf16[2,64,2048]{2,1,0:T(8,128)(2,1)S(1)} %slice.139), channel_id=1, source_target_pairs={{0,6},{2,0},{4,2},{6,4},{1,7},{3,1},{5,3},{7,5},{8,14},{10,8},{12,... | collective-permute-start | bytes 1572872 | tf_op jit(solution)/shard_map/ppermute | solution.py:22
  62.3 7.3 %collective-permute-start.4 = (bf16[512,2048]{1,0:T(8,128)(2,1)S(1)}, bf16[512,2048]{1,0:T(8,128)(2,1)}, u32[]{:S(2)}, u32[]{:S(2)}) collective-permute-start(bf16[512,2048]{1,0:T(8,128)(2,1)S(1)} %bitcast.38), channel_id=1, source_target_pairs={{0,1},{1,0},{2,3},{3,2},{4,5},{5,4},{6,7},{7,6},{8,9},{9,8},{10,11... | collective-permute-start | bytes 6291464 | tf_op jit(solution)/shard_map/ppermute | solution.py:26
  65.7 8.0 %collective-permute-start.5 = (bf16[512,2048]{1,0:T(8,128)(2,1)}, bf16[512,2048]{1,0:T(8,128)(2,1)}, u32[]{:S(2)}, u32[]{:S(2)}) collective-permute-start(bf16[512,2048]{1,0:T(8,128)(2,1)} %bitcast.2.own_ref), channel_id=1, source_target_pairs={{0,1},{1,0},{2,3},{3,2},{4,5},{5,4},{6,7},{7,6},{8,9},{9,8},{10,11... | collective-permute-start | bytes 6291464 | tf_op jit(solution)/shard_map/ppermute | solution.py:26
  66.4 7.3 %copy-start.6 = (bf16[1024,384]{1,0:T(8,128)(2,1)S(1)}, bf16[1024,384]{1,0:T(8,128)(2,1)}, u32[]{:S(2)}) copy-start(bf16[1024,384]{1,0:T(8,128)(2,1)} %cotangent_ref.1) | copy-start | bytes 2359300
  73.7 1.9 %copy-start.4 = (bf16[2048,768]{1,0:T(8,128)(2,1)S(1)}, bf16[2048,768]{1,0:T(8,128)(2,1)}, u32[]{:S(2)}) copy-start(bf16[2048,768]{1,0:T(8,128)(2,1)} %all-gather.2.cloned.1.call-done.up_ref.gate_ref) | copy-start | bytes 9437188
  75.6 11.6 %copy-start.8 = (bf16[1024,2048]{1,0:T(8,128)(2,1)S(1)}, bf16[1024,2048]{1,0:T(8,128)(2,1)}, u32[]{:S(2)}) copy-start(bf16[1024,2048]{1,0:T(8,128)(2,1)} %pad_maximum_fusion) | copy-start | bytes 12582916
  86.0 1.1 copy-start.7
  92.1 1.9 %copy-start.5 = (bf16[2048,768]{1,0:T(8,128)(2,1)S(1)}, bf16[2048,768]{1,0:T(8,128)(2,1)}, u32[]{:S(2)}) copy-start(bf16[2048,768]{1,0:T(8,128)(2,1)} %all-gather.2.cloned.1.call-done.up_ref.gate_ref) | copy-start | bytes 9437188
  98.2 4.5 %collective-permute-start.6 = (bf16[512,2048]{1,0:T(8,128)(2,1)}, bf16[512,2048]{1,0:T(8,128)(2,1)}, u32[]{:S(2)}, u32[]{:S(2)}) collective-permute-start(bf16[512,2048]{1,0:T(8,128)(2,1)} %convolution_convert_fusion.1), channel_id=1, source_target_pairs={{0,1},{1,0},{2,3},{3,2},{4,5},{5,4},{6,7},{7,6},{8,9},{9,8},{10,11... | collective-permute-start | bytes 6291464 | tf_op jit(solution)/shard_map/ppermute | solution.py:26
  106.4 1.4 copy-start.9
  108.7 12.0 %collective-permute-start.7 = (bf16[64,2048]{1,0:T(8,128)(2,1)}, bf16[64,2048]{1,0:T(8,128)(2,1)}, u32[]{:S(2)}, u32[]{:S(2)}) collective-permute-start(bf16[64,2048]{1,0:T(8,128)(2,1)} %get-tuple-element.24), channel_id=1, source_target_pairs={{0,2},{2,4},{4,6},{6,0},{1,3},{3,5},{5,7},{7,1},{8,10},{10,12},{12... | collective-permute-start | bytes 786440 | tf_op jit(solution)/shard_map/ppermute | solution.py:22
  109.1 11.5 %collective-permute-start.9 = (bf16[64,2048]{1,0:T(8,128)(2,1)}, bf16[64,2048]{1,0:T(8,128)(2,1)}, u32[]{:S(2)}, u32[]{:S(2)}) collective-permute-start(bf16[64,2048]{1,0:T(8,128)(2,1)} %get-tuple-element.26), channel_id=1, source_target_pairs={{0,6},{2,0},{4,2},{6,4},{1,7},{3,1},{5,3},{7,5},{8,14},{10,8},{12,... | collective-permute-start | bytes 786440 | tf_op jit(solution)/shard_map/ppermute | solution.py:22
  112.5 17.3 %all-to-all-start.2 = ((f32[8,3,768]{2,1,0:T(4,128)}), f32[8,3,768]{2,1,0:T(4,128)S(1)}, u32[]{:S(2)}, u32[]{:S(2)}) async-start(f32[8,3,768]{2,1,0:T(4,128)} %broadcast_in_dim.9), calls=%async_computation.3 | async-start | bytes 196608 | tf_op jit(solution)/shard_map/all_to_all | solution.py:30
  123.8 38.0 %collective-permute-start.10 = (bf16[128,2048]{1,0:T(8,128)(2,1)}, bf16[128,2048]{1,0:T(8,128)(2,1)}, u32[]{:S(2)}, u32[]{:S(2)}) collective-permute-start(bf16[128,2048]{1,0:T(8,128)(2,1)} %pad_maximum_fusion.2), channel_id=1, source_target_pairs={{0,6},{2,0},{4,2},{6,4},{1,7},{3,1},{5,3},{7,5},{8,14},{10,8},{12,... | collective-permute-start | bytes 1572872 | tf_op jit(solution)/shard_map/ppermute | solution.py:22
  126.1 35.7 %collective-permute-start.8 = (bf16[128,2048]{1,0:T(8,128)(2,1)}, bf16[128,2048]{1,0:T(8,128)(2,1)}, u32[]{:S(2)}, u32[]{:S(2)}) collective-permute-start(bf16[128,2048]{1,0:T(8,128)(2,1)} %pad_maximum_fusion.1), channel_id=1, source_target_pairs={{0,2},{2,4},{4,6},{6,0},{1,3},{3,5},{5,7},{7,1},{8,10},{10,12},{12... | collective-permute-start | bytes 1572872 | tf_op jit(solution)/shard_map/ppermute | solution.py:22
  143.1 12.9 %all-to-all-start.4 = ((f32[4,8,3,768]{3,1,2,0:T(8,128)}), f32[4,8,3,768]{3,1,2,0:T(8,128)S(1)}, u32[]{:S(2)}, u32[]{:S(2)}) async-start(f32[4,8,3,768]{3,1,2,0:T(8,128)} %broadcast_in_dim.11), calls=%async_computation.5 | async-start | bytes 589824 | tf_op jit(solution)/shard_map/all_to_all | solution.py:30
  146.6 9.8 %copy-start.12 = (f32[3,3072]{1,0:T(4,128)S(1)}, f32[3,3072]{1,0:T(4,128)}, u32[]{:S(2)}) copy-start(f32[3,3072]{1,0:T(4,128)} %param.20) | copy-start | bytes 110596
  146.6 10.4 %copy-start.13 = (f32[3,3072]{1,0:T(4,128)S(1)}, f32[3,3072]{1,0:T(4,128)}, u32[]{:S(2)}) copy-start(f32[3,3072]{1,0:T(4,128)} %param.21) | copy-start | bytes 110596
  156.0 12.6 %copy-start.10 = (f32[64,384]{1,0:T(8,128)S(1)}, f32[64,384]{1,0:T(8,128)}, u32[]{:S(2)}) copy-start(f32[64,384]{1,0:T(8,128)} %param.19) | copy-start | bytes 294916
  156.0 12.6 %copy-start.11 = (f32[64,384]{1,0:T(8,128)S(1)}, f32[64,384]{1,0:T(8,128)}, u32[]{:S(2)}) copy-start(f32[64,384]{1,0:T(8,128)} %param.18) | copy-start | bytes 294916
  157.6 10.9 %all-to-all-start.1 = ((bf16[4,64,768]{2,1,0:T(8,128)(2,1)}), bf16[4,64,768]{2,1,0:T(8,128)(2,1)S(1)}, u32[]{:S(2)}, u32[]{:S(2)}) async-start(bf16[4,64,768]{2,1,0:T(8,128)(2,1)} %bitcast.45), calls=%async_computation.2 | async-start | bytes 786432 | tf_op jit(solution)/shard_map/all_to_all | solution.py:30
Sparse Core Ops, SparseCore 0:
  20.1 47.5 all-gather.1
  92.2 47.2 reduce-scatter.1

commit v2 on v1

--- a/solution.py
+++ b/solution.py
@@ -315,13 +315,15 @@
 
     own = sum_to_owner_x(own_z)
     taps_all = taps_all.reshape(group, 3, 2, cols).transpose(2, 1, 0, 3).reshape(2, 3, -1)
+    new_up_taps = up_taps_sum + grad_scale * taps_all[0]
+    new_gate_taps = gate_taps_sum + grad_scale * taps_all[1]
     return (
         hidden,
         input_grad,
         up_grad_sum + grad_scale * own[:, :cols],
         gate_grad_sum + grad_scale * own[:, cols:],
-        up_taps_sum + grad_scale * taps_all[0],
-        gate_taps_sum + grad_scale * taps_all[1],
+        new_up_taps,
+        new_gate_taps,
     )
 
 

time: 178 us -> 178 us (level)
  no operation moved by 1% of the time
where the time goes in v2:
time: 178 us; the launch traced here: 176 us
  waiting for transfers between devices  38.3 us (22%)
  starting transfers between devices  30.8 us (17%)
  blocking collectives  23.5 us (13%)
  local copies, waits for them, and re-layouts  23 us (13%)
  Pallas kernels  19.9 us (11%)
  between operations  14.3 us (8%)
  other arithmetic  13.5 us (8%)
  matrix products  12.8 us (7%)
    all_to_all x2, blocking collectives, exchanged(): return lax.all_to_all(tiles, axis, 0, 0, tiled=True)  23.5 us
    ppermute x8, waiting for transfers between devices, shift(): lax.ppermute(array, axis, [(i, (i + steps) % peers) for i in range(peers)])  22.8 us
    all_to_all x3, starting transfers between devices, exchanged(): return lax.all_to_all(tiles, axis, 0, 0, tiled=True)  15.7 us
    ppermute x8, starting transfers between devices, shift(): lax.ppermute(array, axis, [(i, (i + steps) % peers) for i in range(peers)])  11.3 us
    pallas_call x1, Pallas kernels, grads_of(): pl.pallas_call(grads_kernel, grid=(steps,), in_specs=common_specs(weights...  10.4 us
    unnamed x30, local copies, waits for them, and re-layouts  9.96 us
    pallas_call x1, Pallas kernels, hidden_of(): pl.pallas_call(hidden_kernel, grid=(steps,), in_specs=common_specs(weight...  9.38 us
    all_to_all x3, waiting for transfers between devices, exchanged(): return lax.all_to_all(tiles, axis, 0, 0, tiled=True)  8.11 us
  transfers between devices with their start and end apart: 16, of which 6 were waited for; matrix products, arithmetic and copies ran while one was open for 19% of the time, Pallas kernels for 5%

profile of v2, /device:TPU:1, one launch (start us, length us, event | category | flops | bytes accessed | tf_op | source)
XLA Modules:
  0.0 176.2 jit_solution(16622292728585396582)
XLA Ops:
  7.2 0.0 all-gather.2.cloned.1.call-start
  7.2 0.8 copy-done.2
  8.0 0.8 copy-done.3
  8.8 11.1 %all_to_all.25 = bf16[4,64,768]{2,1,0:T(8,128)(2,1)} all-to-all(bf16[4,64,768]{2,1,0:T(8,128)(2,1)S(1)} %shard_map.155), channel_id=1, replica_groups=mesh['z'=8,'x'=4,'y'=4,'c'=2] {'x'}, dimensions={0} | all-to-all | bytes 786432 | tf_op jit(solution)/shard_map/all_to_all | solution.py:30
  19.9 0.0 all-gather.2.cloned.1.call-update
  20.0 0.0 reduce-scatter.2.cloned.1.call-start
  20.0 1.0 copy-done
  21.0 1.0 copy-done.1
  22.1 0.1 shard_map.154
  22.2 2.3 %collective-permute-start = (bf16[2,128,2048]{2,1,0:T(8,128)(2,1)S(1)}, bf16[2,128,2048]{2,1,0:T(8,128)(2,1)}, u32[]{:S(2)}, u32[]{:S(2)}) collective-permute-start(bf16[2,128,2048]{2,1,0:T(8,128)(2,1)S(1)} %shard_map.154), channel_id=1, source_target_pairs={{0,2},{2,4},{4,6},{6,0},{1,3},{3,5},{5,7},{7,1},{8,10},{10,12},{12... | collective-permute-start | bytes 3145736 | tf_op jit(solution)/shard_map/ppermute | solution.py:22
  24.4 1.5 collective-permute-start.1
  25.9 1.7 broadcast.19.clone
  27.6 0.8 slice_dynamic-update-slice_fusion.2
  28.4 0.2 broadcast.19.clone.1
  28.7 0.1 slice_dynamic-update-slice_fusion.5
  28.8 18.7 %collective-permute-done = bf16[2,128,2048]{2,1,0:T(8,128)(2,1)} collective-permute-done((bf16[2,128,2048]{2,1,0:T(8,128)(2,1)S(1)}, bf16[2,128,2048]{2,1,0:T(8,128)(2,1)}, u32[]{:S(2)}, u32[]{:S(2)}) %collective-permute-start) | collective-permute-done | bytes 1048608 | tf_op jit(solution)/shard_map/ppermute | solution.py:22
  47.5 1.1 slice.137
  48.5 0.1 collective-permute-start.2
  48.6 1.1 slice.139
  49.7 2.7 %collective-permute-start.3 = (bf16[2,64,2048]{2,1,0:T(8,128)(2,1)S(1)}, bf16[2,64,2048]{2,1,0:T(8,128)(2,1)S(1)}, u32[]{:S(2)}, u32[]{:S(2)}) collective-permute-start(bf16[2,64,2048]{2,1,0:T(8,128)(2,1)S(1)} %slice.139), channel_id=1, source_target_pairs={{0,6},{2,0},{4,2},{6,4},{1,7},{3,1},{5,3},{7,5},{8,14},{10,8},{12,... | collective-permute-start | bytes 1572872 | tf_op jit(solution)/shard_map/ppermute | solution.py:22
  52.5 2.1 %slice_dynamic-update-slice_fusion.1 = (bf16[4,128,2048]{2,1,0:T(8,128)(2,1)}, bf16[4,128,2048]{2,1,0:T(8,128)(2,1)S(1)}) fusion(bf16[4,128,2048]{2,1,0:T(8,128)(2,1)} %slice_dynamic-update-slice_fusion.2, s32[]{:T(128)S(6)} %select_n.69, bf16[2,128,2048]{2,1,0:T(8,128)(2,1)} %collective-permute-done, ...), kind=kLoop, calls=%fused_computation.12 | loop fusion | bytes 2097156 | tf_op jit(solution)/shard_map/dynamic_update_slice | solution.py:69
  54.6 2.1 %slice_dynamic-update-slice_fusion = (bf16[4,128,2048]{2,1,0:T(8,128)(2,1)}, bf16[4,128,2048]{2,1,0:T(8,128)(2,1)S(1)}) fusion(bf16[4,128,2048]{2,1,0:T(8,128)(2,1)} %get-tuple-element.30, s32[]{:T(128)S(6)} %select_n.71, bf16[2,128,2048]{2,1,0:T(8,128)(2,1)} %collective-permute-done.1, bf16[4,128,2048]{2,1,0:T(8,128)(2,1)S(1)} %get-tuple-element.31), kind=kLoop, calls=%fused_computation.11 | loop fusion | bytes 2097156 | tf_op jit(solution)/shard_map/dynamic_update_slice | solution.py:69
  56.7 4.1 %collective-permute-done.2 = bf16[2,64,2048]{2,1,0:T(8,128)(2,1)S(1)} collective-permute-done((bf16[2,64,2048]{2,1,0:T(8,128)(2,1)S(1)}, bf16[2,64,2048]{2,1,0:T(8,128)(2,1)S(1)}, u32[]{:S(2)}, u32[]{:S(2)}) %collective-permute-start.2) | collective-permute-done | bytes 524320 | tf_op jit(solution)/shard_map/ppermute | solution.py:22
  60.8 0.8 slice_dynamic-update-slice_fusion.7
  61.6 0.7 slice_dynamic-update-slice_fusion.6
  62.3 3.4 %collective-permute-start.4 = (bf16[512,2048]{1,0:T(8,128)(2,1)S(1)}, bf16[512,2048]{1,0:T(8,128)(2,1)}, u32[]{:S(2)}, u32[]{:S(2)}) collective-permute-start(bf16[512,2048]{1,0:T(8,128)(2,1)S(1)} %bitcast.38), channel_id=1, source_target_pairs={{0,1},{1,0},{2,3},{3,2},{4,5},{5,4},{6,7},{7,6},{8,9},{9,8},{10,11... | collective-permute-start | bytes 6291464 | tf_op jit(solution)/shard_map/ppermute | solution.py:26
  65.7 0.7 fusion.10
  66.4 3.2 %collective-permute-done.4.other_ref = bf16[512,2048]{1,0:T(8,128)(2,1)} collective-permute-done((bf16[512,2048]{1,0:T(8,128)(2,1)S(1)}, bf16[512,2048]{1,0:T(8,128)(2,1)}, u32[]{:S(2)}, u32[]{:S(2)}) %collective-permute-start.4) | collective-permute-done | bytes 2097184 | tf_op jit(solution)/shard_map/ppermute | solution.py:26
  69.6 4.1 %pad_maximum_fusion = bf16[1024,2048]{1,0:T(8,128)(2,1)} fusion(bf16[512,2048]{1,0:T(8,128)(2,1)} %collective-permute-done.4.other_ref, bf16[512,2048]{1,0:T(8,128)(2,1)S(1)} %bitcast.39), kind=kLoop, calls=%fused_computation | loop fusion | flops 8388608 | bytes 8388608 | tf_op jit(solution)/shard_map/concatenate | solution.py:303
  73.7 1.9 %copy-done.4 = bf16[2048,768]{1,0:T(8,128)(2,1)S(1)} copy-done((bf16[2048,768]{1,0:T(8,128)(2,1)S(1)}, bf16[2048,768]{1,0:T(8,128)(2,1)}, u32[]{:S(2)}) %copy-start.4) | copy-done | bytes 3145752
  75.6 10.4 %shard_map.157 = (bf16[1024,768]{1,0:T(8,128)(2,1)S(1)}, f32[3,768]{1,0:T(4,128)S(1)}) custom-call(s32[1]{0:T(128)} %bitcast.core_ref, bf16[512,2048]{1,0:T(8,128)(2,1)S(1)} %bitcast.40, bf16[512,2048]{1,0:T(8,128)(2,1)} %collective-permute-done.4.other_ref, bf16[2048,768]{1,0:T(8,128)(2,1)S(1)} %copy-done.4, bf16[2048,768]{1,0:T(8,128)(2,1)S(1)} %copy-done.4, ...), custom_call_target="tpu_custom_call" | custom-call | flops 3221225472 | bytes 8388608 | tf_op jit(solution)/shard_map/pallas_call | solution.py:219
  86.0 1.1 copy-done.7
  87.2 4.9 %convolution_convert_fusion = bf16[2048,768]{1,0:T(8,128)(2,1)} fusion(bf16[1024,2048]{1,0:T(8,128)(2,1)S(1)} %copy-done.8, bf16[1024,768]{1,0:T(8,128)(2,1)S(1)} %get-tuple-element.17), kind=kOutput, calls=%fused_computation.2 | convolution fusion | flops 3222798336 | bytes 8912896 | tf_op jit(solution)/shard_map/dot_general | solution.py:306
  92.1 0.0 reduce-scatter.2.cloned.1.call-update
  92.1 1.9 %copy-done.5 = bf16[2048,768]{1,0:T(8,128)(2,1)S(1)} copy-done((bf16[2048,768]{1,0:T(8,128)(2,1)S(1)}, bf16[2048,768]{1,0:T(8,128)(2,1)}, u32[]{:S(2)}) %copy-start.5) | copy-done | bytes 3145752
  93.9 4.3 %convolution_convert_fusion.1 = bf16[512,2048]{1,0:T(8,128)(2,1)} fusion(bf16[2048,768]{1,0:T(8,128)(2,1)S(1)} %copy-done.5, bf16[1024,768]{1,0:T(8,128)(2,1)} %copy-done.7), kind=kOutput, calls=%fused_computation.3 | convolution fusion | flops 1611661312 | bytes 6029312 | tf_op jit(solution)/shard_map/dot_general | solution.py:247
  98.2 0.4 collective-permute-start.6
  98.6 4.1 %collective-permute-done.6 = bf16[512,2048]{1,0:T(8,128)(2,1)} collective-permute-done((bf16[512,2048]{1,0:T(8,128)(2,1)}, bf16[512,2048]{1,0:T(8,128)(2,1)}, u32[]{:S(2)}, u32[]{:S(2)}) %collective-permute-start.6) | collective-permute-done | bytes 2097184 | tf_op jit(solution)/shard_map/ppermute | solution.py:26
  102.7 3.7 %add_convert_fusion = bf16[512,2048]{1,0:T(8,128)(2,1)S(1)} fusion(bf16[512,2048]{1,0:T(8,128)(2,1)} %collective-permute-done.6, bf16[2048,768]{1,0:T(8,128)(2,1)S(1)} %copy-done.5, bf16[1024,768]{1,0:T(8,128)(2,1)} %copy-done.7), kind=kOutput, calls=%fused_computation.1 | convolution fusion | flops 1615855616 | bytes 8126464 | tf_op jit(solution)/shard_map/dot_general | solution.py:247
  106.4 1.3 copy-done.9
  107.8 0.9 dynamic-slice_bitcast_fusion.4
  108.7 0.4 collective-permute-start.7
  109.1 2.8 %collective-permute-start.9 = (bf16[64,2048]{1,0:T(8,128)(2,1)}, bf16[64,2048]{1,0:T(8,128)(2,1)}, u32[]{:S(2)}, u32[]{:S(2)}) collective-permute-start(bf16[64,2048]{1,0:T(8,128)(2,1)} %get-tuple-element.26), channel_id=1, source_target_pairs={{0,6},{2,0},{4,2},{6,4},{1,7},{3,1},{5,3},{7,5},{8,14},{10,8},{12,... | collective-permute-start | bytes 786440 | tf_op jit(solution)/shard_map/ppermute | solution.py:22
  111.9 0.7 broadcast_in_dim.9
  112.5 8.1 %all-to-all-start.2 = ((f32[8,3,768]{2,1,0:T(4,128)}), f32[8,3,768]{2,1,0:T(4,128)S(1)}, u32[]{:S(2)}, u32[]{:S(2)}) async-start(f32[8,3,768]{2,1,0:T(4,128)} %broadcast_in_dim.9), calls=%async_computation.3 | async-start | bytes 196608 | tf_op jit(solution)/shard_map/all_to_all | solution.py:30
  120.7 1.3 fusion.5
  122.0 1.8 %pad_maximum_fusion.2 = bf16[128,2048]{1,0:T(8,128)(2,1)} fusion(bf16[64,2048]{1,0:T(8,128)(2,1)S(1)} %get-tuple-element.23, bf16[64,2048]{1,0:T(8,128)(2,1)} %get-tuple-element.25), kind=kLoop, calls=%fused_computation.18 | loop fusion | flops 1048576 | bytes 1048576 | tf_op jit(solution)/shard_map/concatenate | solution.py:264
  123.8 1.5 collective-permute-start.10
  125.3 0.8 pad_maximum_fusion.1
  126.1 3.8 %all-to-all-done.2 = f32[8,3,768]{2,1,0:T(4,128)S(1)} async-done(((f32[8,3,768]{2,1,0:T(4,128)}), f32[8,3,768]{2,1,0:T(4,128)S(1)}, u32[]{:S(2)}, u32[]{:S(2)}) %all-to-all-start.2) | async-done | bytes 73760 | tf_op jit(solution)/shard_map/all_to_all | solution.py:30
  129.9 12.5 %all_to_all.26 = f32[8,3,768]{2,1,0:T(4,128)S(1)} all-to-all(f32[8,3,768]{2,1,0:T(4,128)S(1)} %broadcast_in_dim.10), channel_id=1, replica_groups=mesh['z'=8,'x'=4,'y'=4,'c'=2] {'y','c'}, dimensions={0} | all-to-all | bytes 147456 | tf_op jit(solution)/shard_map/all_to_all | solution.py:30
  142.4 0.7 broadcast_in_dim.11
  143.1 3.5 %all-to-all-start.4 = ((f32[4,8,3,768]{3,1,2,0:T(8,128)}), f32[4,8,3,768]{3,1,2,0:T(8,128)S(1)}, u32[]{:S(2)}, u32[]{:S(2)}) async-start(f32[4,8,3,768]{3,1,2,0:T(8,128)} %broadcast_in_dim.11), calls=%async_computation.5 | async-start | bytes 589824 | tf_op jit(solution)/shard_map/all_to_all | solution.py:30
  146.6 0.0 copy-start.12
  146.6 0.0 copy-start.13
  146.6 9.4 %shard_map.156 = bf16[1024,384]{1,0:T(8,128)(2,1)} custom-call(s32[1]{0:T(128)} %bitcast.core_ref, bf16[512,2048]{1,0:T(8,128)(2,1)} %bitcast.2.own_ref, bf16[512,2048]{1,0:T(8,128)(2,1)} %collective-permute-done.5.other_ref, bf16[2048,768]{1,0:T(8,128)(2,1)S(1)} %copy-done.5, bf16[2048,768]{1,0:T(8,128)(2,1)S(1)} %copy-done.5, ...), custom_call_target="tpu_custom_call" | custom-call | flops 3221225472 | bytes 8388608 | tf_op jit(solution)/shard_map/pallas_call | solution.py:203
  156.1 0.2 fusion.8
  156.4 0.6 add.119
  157.0 0.6 add.120
  157.6 4.2 %all-to-all-start.1 = ((bf16[4,64,768]{2,1,0:T(8,128)(2,1)}), bf16[4,64,768]{2,1,0:T(8,128)(2,1)S(1)}, u32[]{:S(2)}, u32[]{:S(2)}) async-start(bf16[4,64,768]{2,1,0:T(8,128)(2,1)} %bitcast.45), calls=%async_computation.2 | async-start | bytes 786432 | tf_op jit(solution)/shard_map/all_to_all | solution.py:30
  161.8 2.4 %fusion.1 = bf16[128,2048]{1,0:T(8,128)(2,1)} fusion(bf16[128,2048]{1,0:T(8,128)(2,1)} %collective-permute-done.10, bf16[128,2048]{1,0:T(8,128)(2,1)} %collective-permute-done.8, bf16[4,128,2048]{2,1,0:T(8,128)(2,1)} %bitcast.43, s32[]{:T(128)S(6)} %select_n.67), kind=kLoop, calls=%fused_computation.7 | loop fusion | flops 1572864 | bytes 2097156 | tf_op jit(solution)/shard_map/convert_element_type | solution.py:267
  164.2 4.4 %all-to-all-done.1 = bf16[4,64,768]{2,1,0:T(8,128)(2,1)S(1)} async-done(((bf16[4,64,768]{2,1,0:T(8,128)(2,1)}), bf16[4,64,768]{2,1,0:T(8,128)(2,1)S(1)}, u32[]{:S(2)}, u32[]{:S(2)}) %all-to-all-start.1) | async-done | bytes 393248 | tf_op jit(solution)/shard_map/all_to_all | solution.py:30
  168.6 0.1 convert_reduce_fusion
  168.6 0.7 fusion.6
  (38 shorter events, 0.3 us)
Async XLA Ops:
  7.2 66.5 %all-gather.2.cloned.1.call-start = ((), (), s32[]{:S(2)}) async-start(), calls=%async_computation.6 | async-start | bytes 3538944 | tf_op jit(solution)/shard_map/all_gather | solution.py:300
  7.2 0.8 copy-start.2
  8.0 0.8 copy-start.3
  20.0 137.7 %reduce-scatter.2.cloned.1.call-start = ((), (), s32[]{:S(2)}) async-start(), calls=%async_computation.7 | async-start | bytes 3538944 | tf_op jit(solution)/shard_map/reduce_scatter | solution.py:309
  20.0 1.0 copy-start
  21.0 1.0 copy-start.1
  22.2 25.3 %collective-permute-start = (bf16[2,128,2048]{2,1,0:T(8,128)(2,1)S(1)}, bf16[2,128,2048]{2,1,0:T(8,128)(2,1)}, u32[]{:S(2)}, u32[]{:S(2)}) collective-permute-start(bf16[2,128,2048]{2,1,0:T(8,128)(2,1)S(1)} %shard_map.154), channel_id=1, source_target_pairs={{0,2},{2,4},{4,6},{6,0},{1,3},{3,5},{5,7},{7,1},{8,10},{10,12},{12... | collective-permute-start | bytes 3145736 | tf_op jit(solution)/shard_map/ppermute | solution.py:22
  24.4 24.2 %collective-permute-start.1 = (bf16[2,128,2048]{2,1,0:T(8,128)(2,1)S(1)}, bf16[2,128,2048]{2,1,0:T(8,128)(2,1)}, u32[]{:S(2)}, u32[]{:S(2)}) collective-permute-start(bf16[2,128,2048]{2,1,0:T(8,128)(2,1)S(1)} %shard_map.154), channel_id=1, source_target_pairs={{0,6},{2,0},{4,2},{6,4},{1,7},{3,1},{5,3},{7,5},{8,14},{10,8},{12,... | collective-permute-start | bytes 3145736 | tf_op jit(solution)/shard_map/ppermute | solution.py:22
  48.5 12.3 %collective-permute-start.2 = (bf16[2,64,2048]{2,1,0:T(8,128)(2,1)S(1)}, bf16[2,64,2048]{2,1,0:T(8,128)(2,1)S(1)}, u32[]{:S(2)}, u32[]{:S(2)}) collective-permute-start(bf16[2,64,2048]{2,1,0:T(8,128)(2,1)S(1)} %slice.137), channel_id=1, source_target_pairs={{0,2},{2,4},{4,6},{6,0},{1,3},{3,5},{5,7},{7,1},{8,10},{10,12},{12... | collective-permute-start | bytes 1572872 | tf_op jit(solution)/shard_map/ppermute | solution.py:22
  49.7 11.8 %collective-permute-start.3 = (bf16[2,64,2048]{2,1,0:T(8,128)(2,1)S(1)}, bf16[2,64,2048]{2,1,0:T(8,128)(2,1)S(1)}, u32[]{:S(2)}, u32[]{:S(2)}) collective-permute-start(bf16[2,64,2048]{2,1,0:T(8,128)(2,1)S(1)} %slice.139), channel_id=1, source_target_pairs={{0,6},{2,0},{4,2},{6,4},{1,7},{3,1},{5,3},{7,5},{8,14},{10,8},{12,... | collective-permute-start | bytes 1572872 | tf_op jit(solution)/shard_map/ppermute | solution.py:22
  62.3 7.3 %collective-permute-start.4 = (bf16[512,2048]{1,0:T(8,128)(2,1)S(1)}, bf16[512,2048]{1,0:T(8,128)(2,1)}, u32[]{:S(2)}, u32[]{:S(2)}) collective-permute-start(bf16[512,2048]{1,0:T(8,128)(2,1)S(1)} %bitcast.38), channel_id=1, source_target_pairs={{0,1},{1,0},{2,3},{3,2},{4,5},{5,4},{6,7},{7,6},{8,9},{9,8},{10,11... | collective-permute-start | bytes 6291464 | tf_op jit(solution)/shard_map/ppermute | solution.py:26
  65.7 8.0 %collective-permute-start.5 = (bf16[512,2048]{1,0:T(8,128)(2,1)}, bf16[512,2048]{1,0:T(8,128)(2,1)}, u32[]{:S(2)}, u32[]{:S(2)}) collective-permute-start(bf16[512,2048]{1,0:T(8,128)(2,1)} %bitcast.2.own_ref), channel_id=1, source_target_pairs={{0,1},{1,0},{2,3},{3,2},{4,5},{5,4},{6,7},{7,6},{8,9},{9,8},{10,11... | collective-permute-start | bytes 6291464 | tf_op jit(solution)/shard_map/ppermute | solution.py:26
  66.4 7.3 %copy-start.6 = (bf16[1024,384]{1,0:T(8,128)(2,1)S(1)}, bf16[1024,384]{1,0:T(8,128)(2,1)}, u32[]{:S(2)}) copy-start(bf16[1024,384]{1,0:T(8,128)(2,1)} %cotangent_ref.1) | copy-start | bytes 2359300
  73.7 1.9 %copy-start.4 = (bf16[2048,768]{1,0:T(8,128)(2,1)S(1)}, bf16[2048,768]{1,0:T(8,128)(2,1)}, u32[]{:S(2)}) copy-start(bf16[2048,768]{1,0:T(8,128)(2,1)} %all-gather.2.cloned.1.call-done.up_ref.gate_ref) | copy-start | bytes 9437188
  75.6 11.6 %copy-start.8 = (bf16[1024,2048]{1,0:T(8,128)(2,1)S(1)}, bf16[1024,2048]{1,0:T(8,128)(2,1)}, u32[]{:S(2)}) copy-start(bf16[1024,2048]{1,0:T(8,128)(2,1)} %pad_maximum_fusion) | copy-start | bytes 12582916
  86.0 1.1 copy-start.7
  92.1 1.9 %copy-start.5 = (bf16[2048,768]{1,0:T(8,128)(2,1)S(1)}, bf16[2048,768]{1,0:T(8,128)(2,1)}, u32[]{:S(2)}) copy-start(bf16[2048,768]{1,0:T(8,128)(2,1)} %all-gather.2.cloned.1.call-done.up_ref.gate_ref) | copy-start | bytes 9437188
  98.2 4.5 %collective-permute-start.6 = (bf16[512,2048]{1,0:T(8,128)(2,1)}, bf16[512,2048]{1,0:T(8,128)(2,1)}, u32[]{:S(2)}, u32[]{:S(2)}) collective-permute-start(bf16[512,2048]{1,0:T(8,128)(2,1)} %convolution_convert_fusion.1), channel_id=1, source_target_pairs={{0,1},{1,0},{2,3},{3,2},{4,5},{5,4},{6,7},{7,6},{8,9},{9,8},{10,11... | collective-permute-start | bytes 6291464 | tf_op jit(solution)/shard_map/ppermute | solution.py:26
  106.4 1.4 copy-start.9
  108.7 12.0 %collective-permute-start.7 = (bf16[64,2048]{1,0:T(8,128)(2,1)}, bf16[64,2048]{1,0:T(8,128)(2,1)}, u32[]{:S(2)}, u32[]{:S(2)}) collective-permute-start(bf16[64,2048]{1,0:T(8,128)(2,1)} %get-tuple-element.24), channel_id=1, source_target_pairs={{0,2},{2,4},{4,6},{6,0},{1,3},{3,5},{5,7},{7,1},{8,10},{10,12},{12... | collective-permute-start | bytes 786440 | tf_op jit(solution)/shard_map/ppermute | solution.py:22
  109.1 11.5 %collective-permute-start.9 = (bf16[64,2048]{1,0:T(8,128)(2,1)}, bf16[64,2048]{1,0:T(8,128)(2,1)}, u32[]{:S(2)}, u32[]{:S(2)}) collective-permute-start(bf16[64,2048]{1,0:T(8,128)(2,1)} %get-tuple-element.26), channel_id=1, source_target_pairs={{0,6},{2,0},{4,2},{6,4},{1,7},{3,1},{5,3},{7,5},{8,14},{10,8},{12,... | collective-permute-start | bytes 786440 | tf_op jit(solution)/shard_map/ppermute | solution.py:22
  112.5 17.3 %all-to-all-start.2 = ((f32[8,3,768]{2,1,0:T(4,128)}), f32[8,3,768]{2,1,0:T(4,128)S(1)}, u32[]{:S(2)}, u32[]{:S(2)}) async-start(f32[8,3,768]{2,1,0:T(4,128)} %broadcast_in_dim.9), calls=%async_computation.3 | async-start | bytes 196608 | tf_op jit(solution)/shard_map/all_to_all | solution.py:30
  123.8 38.0 %collective-permute-start.10 = (bf16[128,2048]{1,0:T(8,128)(2,1)}, bf16[128,2048]{1,0:T(8,128)(2,1)}, u32[]{:S(2)}, u32[]{:S(2)}) collective-permute-start(bf16[128,2048]{1,0:T(8,128)(2,1)} %pad_maximum_fusion.2), channel_id=1, source_target_pairs={{0,6},{2,0},{4,2},{6,4},{1,7},{3,1},{5,3},{7,5},{8,14},{10,8},{12,... | collective-permute-start | bytes 1572872 | tf_op jit(solution)/shard_map/ppermute | solution.py:22
  126.1 35.7 %collective-permute-start.8 = (bf16[128,2048]{1,0:T(8,128)(2,1)}, bf16[128,2048]{1,0:T(8,128)(2,1)}, u32[]{:S(2)}, u32[]{:S(2)}) collective-permute-start(bf16[128,2048]{1,0:T(8,128)(2,1)} %pad_maximum_fusion.1), channel_id=1, source_target_pairs={{0,2},{2,4},{4,6},{6,0},{1,3},{3,5},{5,7},{7,1},{8,10},{10,12},{12... | collective-permute-start | bytes 1572872 | tf_op jit(solution)/shard_map/ppermute | solution.py:22
  143.1 12.9 %all-to-all-start.4 = ((f32[4,8,3,768]{3,1,2,0:T(8,128)}), f32[4,8,3,768]{3,1,2,0:T(8,128)S(1)}, u32[]{:S(2)}, u32[]{:S(2)}) async-start(f32[4,8,3,768]{3,1,2,0:T(8,128)} %broadcast_in_dim.11), calls=%async_computation.5 | async-start | bytes 589824 | tf_op jit(solution)/shard_map/all_to_all | solution.py:30
  146.6 9.8 %copy-start.12 = (f32[3,3072]{1,0:T(4,128)S(1)}, f32[3,3072]{1,0:T(4,128)}, u32[]{:S(2)}) copy-start(f32[3,3072]{1,0:T(4,128)} %param.20) | copy-start | bytes 110596
  146.6 10.4 %copy-start.13 = (f32[3,3072]{1,0:T(4,128)S(1)}, f32[3,3072]{1,0:T(4,128)}, u32[]{:S(2)}) copy-start(f32[3,3072]{1,0:T(4,128)} %param.21) | copy-start | bytes 110596
  156.0 12.6 %copy-start.10 = (f32[64,384]{1,0:T(8,128)S(1)}, f32[64,384]{1,0:T(8,128)}, u32[]{:S(2)}) copy-start(f32[64,384]{1,0:T(8,128)} %param.19) | copy-start | bytes 294916
  156.0 12.6 %copy-start.11 = (f32[64,384]{1,0:T(8,128)S(1)}, f32[64,384]{1,0:T(8,128)}, u32[]{:S(2)}) copy-start(f32[64,384]{1,0:T(8,128)} %param.18) | copy-start | bytes 294916
  157.6 10.9 %all-to-all-start.1 = ((bf16[4,64,768]{2,1,0:T(8,128)(2,1)}), bf16[4,64,768]{2,1,0:T(8,128)(2,1)S(1)}, u32[]{:S(2)}, u32[]{:S(2)}) async-start(bf16[4,64,768]{2,1,0:T(8,128)(2,1)} %bitcast.45), calls=%async_computation.2 | async-start | bytes 786432 | tf_op jit(solution)/shard_map/all_to_all | solution.py:30
Sparse Core Ops, SparseCore 0:
  20.1 47.5 all-gather.1
  92.2 47.2 reduce-scatter.1
